TPU v7x, 256 devices: a whole 4x4x8 slice. The times are simulated.
256 devices in a mesh: sp: 64 (over z, x, core), tp: 4 (over y).
Axes of the slice: x: 4, y: 4, z: 8, core: 2. Of those that a mesh axis runs over, the one named last changes fastest.
Arguments:
- queries: bfloat16 [65536, 2048], P('sp', 'tp'), may hold values from -16 to 16
- key_rows: bfloat16 [65536, 512], P('sp', 'tp'), may hold values from -16 to 16
- value_rows: bfloat16 [65536, 512], P('sp', 'tp'), may hold values from -6 to 6
- doc_ids: int32 [65536], P('sp'), may hold values from 0 to 31, never falling along the last dimension, each value on 1 to 4096 neighbouring positions
- sink_logit: float32 [32], P('tp'), may hold values from 3 to 7
- residual: bfloat16 [65536, 2048], P(('sp', 'tp')), may hold values from -6 to 6
- out_weight: bfloat16 [2048, 2048], P('tp'), may hold values from -3.5 to 3.5
- norm_gain: float32 [2048], replicated, may hold values from 0.1 to 1.9
- gate_weight: bfloat16 [64, 2048, 512], P('sp'), may hold values from -0.125 to 0.125
- up_weight: bfloat16 [64, 2048, 512], P('sp'), may hold values from -0.125 to 0.125
- down_weight: bfloat16 [64, 512, 2048], P('sp'), may hold values from -0.25 to 0.25
- routes: int32 [65536, 2], P(('sp', 'tp')), may hold values from 0 to 63, as said below
- route_weights: float32 [65536, 2], P(('sp', 'tp')), may hold values from 0.2 to 0.8
Outputs:
- mixed: bfloat16 [65536, 2048], P(('sp', 'tp'))
Inputs may be any that keep to these rules, and one draw needn't show every extreme that they name: `doc_ids`: never falls along the positions. `routes`: each aligned block of 256 rows names every expert exactly 8 times; the experts of one row differ and lie in one group of 16 consecutive numbers.
All inputs are finite; a program needn't handle non-finite values.
Results may differ from a plain program's by a relative error of at most 0.012.
Values may be sent and summed in bfloat16 or wider, within the bound.
A program may use at most 128 MiB of HBM per device.

v0:
```python
import jax
import jax.numpy as jnp
from jax import lax
from jax.sharding import PartitionSpec as P

HD = 64
WINDOW = 128


neg_fill = -1e30
eps_norm = 1e-06


def extended(block, sides, width):
    for axis, dim in sides:
        count = lax.axis_size(axis)
        forward = [(i, i + 1) for i in range(count - 1)]
        backward = [(target, source) for source, target in forward]
        low = lax.ppermute(
            lax.slice_in_dim(block, block.shape[dim] - width, None, axis=dim), axis, forward
        )
        high = lax.ppermute(lax.slice_in_dim(block, 0, width, axis=dim), axis, backward)
        block = jnp.concatenate([low, block, high], axis=dim)
    return block


def attend(
    query_part,
    key_part,
    value_part,
    query_docs,
    key_docs,
    query_start,
    key_start,
    sink_logit,
    extent,
):
    query_count = query_part.shape[0]
    key_count = key_part.shape[0]
    groups = key_part.shape[1] // HD
    head_ratio = sink_logit.shape[0] // groups
    query_heads = query_part.reshape(query_count, groups, head_ratio, HD)
    key_heads = key_part.reshape(key_count, groups, HD)
    value_heads = value_part.reshape(key_count, groups, HD)
    scores = jnp.einsum(
        "qgrd,kgd->grqk", query_heads, key_heads, preferred_element_type=jnp.float32
    ) * HD ** (-0.5)
    query_pos = query_start + jnp.arange(query_count, dtype=jnp.int32)
    key_pos = key_start + jnp.arange(key_count, dtype=jnp.int32)
    inside = (key_pos >= 0) & (key_pos < extent)
    allowed = (
        (jnp.abs(query_pos[:, None] - key_pos[None, :]) <= WINDOW)
        & (query_docs[:, None] == key_docs[None, :])
        & inside[None, :]
    )
    masked = jnp.where(allowed[None, None], scores, neg_fill)
    sink_col = sink_logit.reshape(groups, head_ratio)[:, :, None, None]
    row_top = jnp.maximum(jnp.max(masked, axis=3, keepdims=True), sink_col)
    exponent = jnp.where(allowed[None, None], jnp.exp(masked - row_top), 0.0)
    denominator = jnp.sum(exponent, axis=3, keepdims=True) + jnp.exp(sink_col - row_top)
    attn_weight = (exponent / denominator).astype(jnp.bfloat16)
    attended = jnp.einsum(
        "grqk,kgd->qgrd", attn_weight, value_heads, preferred_element_type=jnp.float32
    )
    return attended.astype(jnp.bfloat16).reshape(query_count, -1)


def fetch_margins(key_rows, value_rows, doc_float):
    return (
        extended(key_rows, (("sp", 0),), WINDOW),
        extended(value_rows, (("sp", 0),), WINDOW),
        extended(doc_float, (("sp", 0),), WINDOW),
    )


def per_device(
    queries,
    key_rows,
    value_rows,
    doc_ids,
    sink_logit,
    residual,
    out_weight,
    norm_gain,
    gate_weight,
    up_weight,
    down_weight,
    routes,
    route_weights,
):
    local_rows = queries.shape[0]
    anchor = lax.axis_index("sp") * local_rows
    extent = local_rows * lax.axis_size("sp")
    doc_float = doc_ids.astype(jnp.bfloat16)
    block_rows = min(512, local_rows)
    padded_keys, padded_values, padded_docs = fetch_margins(key_rows, value_rows, doc_float)
    block_parts = []
    for row_start in range(0, local_rows, block_rows):
        key_end = row_start + block_rows + 2 * WINDOW
        block_parts.append(
            attend(
                queries[row_start : row_start + block_rows],
                padded_keys[row_start:key_end],
                padded_values[row_start:key_end],
                doc_float[row_start : row_start + block_rows],
                padded_docs[row_start:key_end],
                anchor + row_start,
                anchor + row_start - WINDOW,
                sink_logit,
                extent,
            )
        )
    attended = jnp.concatenate(block_parts, axis=0)
    regrouped = lax.all_to_all(attended, "tp", split_axis=0, concat_axis=1, tiled=True)
    shard_rows = out_weight.shape[0]
    initial = jnp.zeros((regrouped.shape[0], out_weight.shape[1]), jnp.float32)
    running = initial
    weight_piece = lax.all_gather(out_weight, "tp", axis=0, tiled=True)
    for shard_index in range(weight_piece.shape[0] // shard_rows):
        columns = lax.dynamic_slice_in_dim(regrouped, shard_index * shard_rows, shard_rows, 1)
        partial_value = jnp.dot(
            columns,
            weight_piece[shard_index * shard_rows : (shard_index + 1) * shard_rows],
            preferred_element_type=jnp.float32,
        )
        running = running + partial_value.astype(jnp.bfloat16).astype(jnp.float32)
    stream = (residual.astype(jnp.float32) + running).astype(jnp.bfloat16)
    stream_f = stream.astype(jnp.float32)
    scale = lax.rsqrt(jnp.mean(stream_f * stream_f, axis=1, keepdims=True) + eps_norm)
    normed = (stream_f * scale * norm_gain[None, :]).astype(jnp.bfloat16)
    home_rows = normed.shape[0]
    width = normed.shape[1]
    route_count = routes.shape[1]
    expert_count = lax.axis_size("sp") * gate_weight.shape[0]
    capacity = route_count * home_rows // expert_count
    flat_routes = routes.reshape(-1)
    one_hot = (flat_routes[:, None] == jnp.arange(expert_count, dtype=jnp.int32)[None, :]).astype(
        jnp.int32
    )
    earlier = jnp.cumsum(one_hot, axis=0) - one_hot
    slot_rank = jnp.sum(earlier * one_hot, axis=1)
    slot_index = flat_routes * capacity + slot_rank
    source_row = (
        jnp.zeros((expert_count * capacity,), jnp.int32)
        .at[slot_index]
        .set(jnp.arange(home_rows * route_count, dtype=jnp.int32) // route_count)
    )
    outgoing = normed[source_row].reshape(expert_count, capacity, width)
    incoming = lax.all_to_all(outgoing, "sp", split_axis=0, concat_axis=0, tiled=True)
    flat_rows = incoming.reshape(-1, width)
    gate_act = jnp.dot(flat_rows, gate_weight[0], preferred_element_type=jnp.float32)
    up_act = jnp.dot(flat_rows, up_weight[0], preferred_element_type=jnp.float32)
    hidden = (jax.nn.silu(gate_act) * up_act).astype(jnp.bfloat16)
    produced = jnp.dot(hidden, down_weight[0], preferred_element_type=jnp.float32).astype(
        jnp.bfloat16
    )
    returned = lax.all_to_all(
        produced.reshape(incoming.shape), "sp", split_axis=0, concat_axis=0, tiled=True
    )
    route_out = returned.reshape(-1, width)[slot_index].reshape(home_rows, route_count, width)
    weighted = jnp.sum(route_weights[:, :, None] * route_out.astype(jnp.float32), axis=1)
    return (stream_f + weighted).astype(jnp.bfloat16)


def solution(mesh):
    return jax.shard_map(
        per_device,
        mesh=mesh,
        in_specs=(
            P("sp", "tp"),
            P("sp", "tp"),
            P("sp", "tp"),
            P("sp"),
            P("tp"),
            P(("sp", "tp"), None),
            P("tp", None),
            P(),
            P("sp", None, None),
            P("sp", None, None),
            P("sp", None, None),
            P(("sp", "tp"), None),
            P(("sp", "tp"), None),
        ),
        out_specs=P(("sp", "tp"), None),
        check_vma=False,
    )
```

profile of v0, /device:TPU:2, one launch (start us, length us, event | category | flops | bytes accessed | tf_op | source)
XLA Modules:
  0.0 280.8 jit_solution(16703556512398380717)
XLA Ops:
  7.9 1.9 collective-permute-start.1
  9.9 3.6 %collective-permute-start.4 = (bf16[128]{0:T(256)(128)(2,1)}, bf16[128]{0:T(256)(128)(2,1)}, u32[]{:S(2)}, u32[]{:S(2)}) collective-permute-start(bf16[128]{0:T(256)(128)(2,1)} %get-tuple-element.18), channel_id=1, source_target_pairs={{4,0},{8,4},{12,8},{16,12},{20,16},{24,20},{28,24},{32,28},{36,32}... | collective-permute-start | bytes 776 | tf_op jit(solution)/shard_map/ppermute | solution.py:22
  16.8 3.6 %collective-permute-start.5 = (bf16[128,128]{1,0:T(8,128)(2,1)}, bf16[128,128]{1,0:T(8,128)(2,1)S(1)}, u32[]{:S(2)}, u32[]{:S(2)}) collective-permute-start(bf16[128,128]{1,0:T(8,128)(2,1)} %get-tuple-element.10), channel_id=1, source_target_pairs={{4,0},{8,4},{12,8},{16,12},{20,16},{24,20},{28,24},{32,28},{36,32}... | collective-permute-start | bytes 98312 | tf_op jit(solution)/shard_map/ppermute | solution.py:22
  34.8 3.6 %collective-permute-start.3 = (bf16[128,128]{1,0:T(8,128)(2,1)}, bf16[128,128]{1,0:T(8,128)(2,1)S(1)}, u32[]{:S(2)}, u32[]{:S(2)}) collective-permute-start(bf16[128,128]{1,0:T(8,128)(2,1)} %get-tuple-element.14), channel_id=1, source_target_pairs={{4,0},{8,4},{12,8},{16,12},{20,16},{24,20},{28,24},{32,28},{36,32}... | collective-permute-start | bytes 98312 | tf_op jit(solution)/shard_map/ppermute | solution.py:22
  39.1 2.3 fusion.33
  50.2 3.1 %fusion = (f32[2,4,512]{2,1,0:T(4,128)S(1)}, f32[2,768,512,4]{2,1,3,0:T(8,128)S(1)}) fusion(pred[512,768]{0,1:T(8,128)(4,1)S(1)} %get-tuple-element.30, bf16[768,2,64,1]{0,2,3,1:T(8,128)(2,1)} %bitcast.124, bf16[512,2,4,64]{0,3,2,1:T(8,128)(2,1)S(1)} %bitcast.121), kind=kOutput, calls=%fused_computation.9 | convolution fusion | flops 412086272 | bytes 13713408 | tf_op jit(solution)/shard_map/qgrd,kgd->grqk/dot_general | solution.py:45
  53.4 6.6 %fusion.1 = (f32[2,4,512]{2,1,0:T(4,128)S(1)}, f32[2,768,512,4]{2,1,3,0:T(8,128)}) fusion(pred[512,768]{0,1:T(8,128)(4,1)S(1)} %get-tuple-element.29, bf16[768,2,64,1]{0,2,3,1:T(8,128)(2,1)S(1)} %bitcast.123, bf16[512,2,4,64]{0,3,2,1:T(8,128)(2,1)S(1)} %bitcast.122), kind=kOutput, calls=%fused_computation.10 | convolution fusion | flops 412086272 | bytes 13713408 | tf_op jit(solution)/shard_map/qgrd,kgd->grqk/dot_general | solution.py:45
  60.0 3.1 %fusion.2 = f32[2,4,512]{2,1,0:T(4,128)S(1)} fusion(f32[2,768,512,4]{2,1,3,0:T(8,128)S(1)} %get-tuple-element.24, f32[2,4,512]{2,1,0:T(4,128)S(1)} %broadcast_maximum_fusion.1, pred[512,768]{0,1:T(8,128)(4,1)S(1)} %get-tuple-element.30), kind=kLoop, calls=%fused_computation.11 | loop fusion | flops 15724544 | bytes 13008896 | tf_op jit(solution)/shard_map/reduce_sum | solution.py:60
  63.2 4.7 %fusion.46 = bf16[2,64,4,512]{3,1,2,0:T(8,128)(2,1)} fusion(bf16[768,2,64,1]{0,2,3,1:T(8,128)(2,1)S(1)} %bitcast.127, f32[2,768,512,4]{2,1,3,0:T(8,128)S(1)} %get-tuple-element.24, f32[2,4,512]{2,1,0:T(4,128)S(1)} %get-tuple-element.21, f32[2,4,512]{2,1,0:T(4,128)S(1)} %broadcast_maximum_fusion.1, pred[512,768]{0,1:T(8,128)(4,1)S(1)} %get-tuple-element.30), kind=kOutput, calls=%fused_computation.58 | convolution fusion | flops 421789696 | bytes 13729792 | tf_op jit(solution)/shard_map/grqk,kgd->qgrd/dot_general | solution.py:62
  69.3 6.9 %fusion.3 = f32[2,4,512]{2,1,0:T(4,128)S(1)} fusion(f32[2,768,512,4]{2,1,3,0:T(8,128)} %get-tuple-element.26, f32[2,4,512]{2,1,0:T(4,128)S(1)} %get-tuple-element.22, pred[512,768]{0,1:T(8,128)(4,1)S(1)} %get-tuple-element.29), kind=kLoop, calls=%fused_computation.12 | loop fusion | flops 15724544 | bytes 13008896 | tf_op jit(solution)/shard_map/reduce_sum | solution.py:60
  77.8 4.6 %fusion.45 = bf16[2,64,4,512]{3,1,2,0:T(8,128)(2,1)} fusion(bf16[768,2,64,1]{0,2,3,1:T(8,128)(2,1)S(1)} %bitcast.128, f32[2,768,512,4]{2,1,3,0:T(8,128)S(1)} %copy-done.1, f32[2,4,512]{2,1,0:T(4,128)S(1)} %exponential_add_fusion, f32[2,4,512]{2,1,0:T(4,128)S(1)} %get-tuple-element.22, pred[512,768]{0,1:T(8,128)(4,1)S(1)} %get-tuple-element.29), kind=kOutput, calls=%fused_computation.57 | convolution fusion | flops 421789696 | bytes 13729792 | tf_op jit(solution)/shard_map/grqk,kgd->qgrd/dot_general | solution.py:62
  84.7 4.6 %all-to-all-start = ((bf16[4,256,512]{2,1,0:T(8,128)(2,1)}), bf16[4,256,512]{2,1,0:T(8,128)(2,1)S(1)}, u32[]{:S(2)}, u32[]{:S(2)}) async-start(bf16[4,256,512]{2,1,0:T(8,128)(2,1)} %bitcast.120), calls=%async_computation | async-start | bytes 2097152 | tf_op jit(solution)/shard_map/all_to_all | solution.py:114
  89.5 2.4 scatter_custom_fusion
  92.0 16.9 %all-to-all-done = bf16[4,256,512]{2,1,0:T(8,128)(2,1)S(1)} async-done(((bf16[4,256,512]{2,1,0:T(8,128)(2,1)}), bf16[4,256,512]{2,1,0:T(8,128)(2,1)S(1)}, u32[]{:S(2)}, u32[]{:S(2)}) %all-to-all-start) | async-done | bytes 1048608 | tf_op jit(solution)/shard_map/all_to_all | solution.py:114
  111.4 2.5 fusion.13
  113.9 2.9 %fusion.14 = f32[256,2048]{1,0:T(8,128)S(1)} fusion(bf16[2048,2048]{1,0:T(8,128)(2,1)} %all-gather.2.cloned.1.call-done, bf16[256,2048]{0,1:T(8,128)(2,1)S(1)} %bitcast.116), kind=kOutput, calls=%fused_computation.32 | convolution fusion | flops 537919488 | bytes 4456448 | tf_op jit(solution)/shard_map/dot_general | solution.py:121
  120.5 3.3 %gather_fusion = bf16[512,2048]{1,0:T(8,128)(2,1)} fusion(bf16[256,2048]{1,0:T(8,128)(2,1)S(1)} %fusion.18, s32[1024]{0:T(1024)S(1)} %pad_clamp_fusion.1), kind=kCustom, calls=%fused_computation | custom fusion | bytes 4196352 | tf_op jit(solution)/shard_map/gather | solution.py:148
  123.7 61.9 %all_to_all.29 = bf16[64,8,2048]{2,1,0:T(8,128)(2,1)S(1)} all-to-all(bf16[64,8,2048]{2,1,0:T(8,128)(2,1)} %bitcast.114), channel_id=1, replica_groups=mesh['sp'=64,'tp'=4] {'sp'}, dimensions={0} | all-to-all | bytes 4194304 | tf_op jit(solution)/shard_map/all_to_all | solution.py:149
  188.2 6.0 %fusion.6 = bf16[64,8,2048]{2,1,0:T(8,128)(2,1)} fusion(bf16[1,512,2048]{2,1,0:T(8,128)(2,1)S(1)} %copy-done, bf16[1,2048,512]{2,1,0:T(8,128)(2,1)} %param.22, bf16[64,8,2048]{2,1,0:T(8,128)(2,1)} %copy-done.6, f32[512,512]{1,0:T(8,128)S(1)} %fusion.27), kind=kOutput, calls=%fused_computation.20 | convolution fusion | flops 2150105088 | bytes 9437184 | tf_op jit(solution)/shard_map/dot_general | solution.py:154
  194.2 5.8 %all-to-all-start.2 = ((bf16[64,8,2048]{2,1,0:T(8,128)(2,1)}), bf16[64,8,2048]{2,1,0:T(8,128)(2,1)}, u32[]{:S(2)}, u32[]{:S(2)}) async-start(bf16[64,8,2048]{2,1,0:T(8,128)(2,1)} %fusion.6), calls=%async_computation.2 | async-start | bytes 4194304 | tf_op jit(solution)/shard_map/all_to_all | solution.py:157
  200.1 51.0 %all-to-all-done.2 = bf16[64,8,2048]{2,1,0:T(8,128)(2,1)} async-done(((bf16[64,8,2048]{2,1,0:T(8,128)(2,1)}), bf16[64,8,2048]{2,1,0:T(8,128)(2,1)}, u32[]{:S(2)}, u32[]{:S(2)}) %all-to-all-start.2) | async-done | bytes 2097184 | tf_op jit(solution)/shard_map/all_to_all | solution.py:157
  251.1 7.1 %gather_fusion.1 = bf16[512,2048]{1,0:T(8,128)(2,1)} fusion(bf16[512,2048]{1,0:T(8,128)(2,1)} %bitcast.32, s32[1024]{0:T(1024)S(1)} %pad_clamp_fusion), kind=kCustom, calls=%fused_computation.1 | custom fusion | bytes 4196352 | tf_op jit(solution)/shard_map/gather | solution.py:160
  258.2 5.4 %reshape.312 = f32[256,2,2048]{2,1,0:T(2,128)} reshape(bf16[512,2048]{1,0:T(8,128)(2,1)} %gather_fusion.1) | data formatting | bytes 6291456 | tf_op jit(solution)/shard_map/convert_element_type | solution.py:161
  263.7 9.0 %multiply_reduce_fusion = f32[256,2048]{1,0:T(8,128)S(1)} fusion(f32[256,2,2048]{2,1,0:T(2,128)} %reshape.312, f32[256,2]{1,0:T(8,128)S(1)} %copy.47), kind=kLoop, calls=%fused_computation.15 | loop fusion | flops 1572864 | bytes 6293504 | tf_op jit(solution)/shard_map/reduce_sum | solution.py:161
  (117 shorter events, 44.2 us)
Async XLA Ops:
  6.5 181.7 %copy-start = (bf16[1,512,2048]{2,1,0:T(8,128)(2,1)S(1)}, bf16[1,512,2048]{2,1,0:T(8,128)(2,1)}, u32[]{:S(2)}) copy-start(bf16[1,512,2048]{2,1,0:T(8,128)(2,1)} %param.23) | copy-start | bytes 6291460
  6.5 17.3 %copy-start.20 = (s32[256,2]{0,1:T(2,128)S(1)}, s32[256,2]{0,1:T(2,128)}, u32[]{:S(2)}) copy-start(s32[256,2]{0,1:T(2,128)} %param.24) | copy-start | bytes 6148
  6.5 104.9 %all-gather.2.cloned.1.call-start = ((), (), s32[]{:S(2)}) async-start(), calls=%async_computation.3 | async-start | bytes 10485760 | tf_op jit(solution)/shard_map/all_gather | solution.py:118
  7.4 19.9 %copy-start.25 = (f32[8]{0:T(128)S(1)}, f32[8]{0:T(128)}, u32[]{:S(2)}) copy-start(f32[8]{0:T(128)} %param.17) | copy-start | bytes 100
  7.9 26.3 %collective-permute-start.1 = (bf16[128]{0:T(256)(128)(2,1)S(1)}, bf16[128]{0:T(256)(128)(2,1)S(1)}, u32[]{:S(2)}, u32[]{:S(2)}) collective-permute-start(bf16[128]{0:T(256)(128)(2,1)S(1)} %get-tuple-element.17), channel_id=1, source_target_pairs={{0,4},{4,8},{8,12},{12,16},{16,20},{20,24},{24,28},{28,32},{32,36}... | collective-permute-start | bytes 776 | tf_op jit(solution)/shard_map/ppermute | solution.py:19
  9.9 28.5 %collective-permute-start.4 = (bf16[128]{0:T(256)(128)(2,1)}, bf16[128]{0:T(256)(128)(2,1)}, u32[]{:S(2)}, u32[]{:S(2)}) collective-permute-start(bf16[128]{0:T(256)(128)(2,1)} %get-tuple-element.18), channel_id=1, source_target_pairs={{4,0},{8,4},{12,8},{16,12},{20,16},{24,20},{28,24},{32,28},{36,32}... | collective-permute-start | bytes 776 | tf_op jit(solution)/shard_map/ppermute | solution.py:22
  14.9 26.5 %collective-permute-start.2 = (bf16[128,128]{1,0:T(8,128)(2,1)}, bf16[128,128]{1,0:T(8,128)(2,1)S(1)}, u32[]{:S(2)}, u32[]{:S(2)}) collective-permute-start(bf16[128,128]{1,0:T(8,128)(2,1)} %get-tuple-element.9), channel_id=1, source_target_pairs={{0,4},{4,8},{8,12},{12,16},{16,20},{20,24},{24,28},{28,32},{32,36}... | collective-permute-start | bytes 98312 | tf_op jit(solution)/shard_map/ppermute | solution.py:19
  16.8 24.6 %collective-permute-start.5 = (bf16[128,128]{1,0:T(8,128)(2,1)}, bf16[128,128]{1,0:T(8,128)(2,1)S(1)}, u32[]{:S(2)}, u32[]{:S(2)}) collective-permute-start(bf16[128,128]{1,0:T(8,128)(2,1)} %get-tuple-element.10), channel_id=1, source_target_pairs={{4,0},{8,4},{12,8},{16,12},{20,16},{24,20},{28,24},{32,28},{36,32}... | collective-permute-start | bytes 98312 | tf_op jit(solution)/shard_map/ppermute | solution.py:22
  21.9 24.8 %collective-permute-start = (bf16[128,128]{1,0:T(8,128)(2,1)}, bf16[128,128]{1,0:T(8,128)(2,1)S(1)}, u32[]{:S(2)}, u32[]{:S(2)}) collective-permute-start(bf16[128,128]{1,0:T(8,128)(2,1)} %get-tuple-element.13), channel_id=1, source_target_pairs={{0,4},{4,8},{8,12},{12,16},{16,20},{20,24},{24,28},{28,32},{32,36}... | collective-permute-start | bytes 98312 | tf_op jit(solution)/shard_map/ppermute | solution.py:19
  29.2 9.9 %copy-start.9 = (s32[64,4,128]{2,0,1:T(8,128)}, s32[64,4,128]{2,0,1:T(8,128)S(1)}, u32[]{:S(2)}) copy-start(s32[64,4,128]{2,0,1:T(8,128)S(1)} %reduce-window.6) | copy-start | bytes 393220
  33.3 16.9 %copy-start.7 = (bf16[512,512]{0,1:T(8,128)(2,1)S(1)}, bf16[512,512]{0,1:T(8,128)(2,1)}, u32[]{:S(2)}) copy-start(bf16[512,512]{0,1:T(8,128)(2,1)} %copy.38) | copy-start | bytes 1572868
  33.4 20.0 %copy-start.15 = (s32[64,5]{0,1:T(8,128)}, s32[64,5]{0,1:T(8,128)S(1)}, u32[]{:S(2)}) copy-start(s32[64,5]{0,1:T(8,128)S(1)} %reduce-window.9) | copy-start | bytes 3844
  34.8 11.9 %collective-permute-start.3 = (bf16[128,128]{1,0:T(8,128)(2,1)}, bf16[128,128]{1,0:T(8,128)(2,1)S(1)}, u32[]{:S(2)}, u32[]{:S(2)}) collective-permute-start(bf16[128,128]{1,0:T(8,128)(2,1)} %get-tuple-element.14), channel_id=1, source_target_pairs={{4,0},{8,4},{12,8},{16,12},{20,16},{24,20},{28,24},{32,28},{36,32}... | collective-permute-start | bytes 98312 | tf_op jit(solution)/shard_map/ppermute | solution.py:22
  63.2 5.9 %copy-start.12 = (bf16[768,128]{1,0:T(8,128)(2,1)S(1)}, bf16[768,128]{1,0:T(8,128)(2,1)}, u32[]{:S(2)}) copy-start(bf16[768,128]{1,0:T(8,128)(2,1)} %get-tuple-element.12) | copy-start | bytes 589828
  69.3 8.5 %copy-start.1 = (f32[2,768,512,4]{2,1,3,0:T(8,128)S(1)}, f32[2,768,512,4]{2,1,3,0:T(8,128)}, u32[]{:S(2)}) copy-start(f32[2,768,512,4]{2,1,3,0:T(8,128)} %get-tuple-element.26) | copy-start | bytes 37748740
  83.7 5.7 %slice-start = ((s32[64,5]{0,1:T(8,128)}), s32[64,4]{0,1:T(4,128)S(1)}, s32[]{:S(2)}) async-start(s32[64,5]{0,1:T(8,128)} %copy-done.15), calls=%async_computation.4 | async-start | bytes 4096 | tf_op jit(solution)/shard_map/slice.1
  83.7 5.7 %copy-start.18 = (s32[512]{0:T(512)S(1)}, s32[512]{0:T(512)}, u32[]{:S(2)}) copy-start(s32[512]{0:T(512)} %eq.65) | copy-start | bytes 6148
  83.7 5.8 %copy-start.19 = (s32[512,1]{0,1:T(1,128)S(1)}, s32[512,1]{0,1:T(1,128)}, u32[]{:S(2)}) copy-start(s32[512,1]{0,1:T(1,128)} %mul.81) | copy-start | bytes 6148
  84.7 24.2 %all-to-all-start = ((bf16[4,256,512]{2,1,0:T(8,128)(2,1)}), bf16[4,256,512]{2,1,0:T(8,128)(2,1)S(1)}, u32[]{:S(2)}, u32[]{:S(2)}) async-start(bf16[4,256,512]{2,1,0:T(8,128)(2,1)} %bitcast.120), calls=%async_computation | async-start | bytes 2097152 | tf_op jit(solution)/shard_map/all_to_all | solution.py:114
  111.4 5.3 %copy-start.4 = (bf16[2048,2048]{1,0:T(8,128)(2,1)S(1)}, bf16[2048,2048]{1,0:T(8,128)(2,1)}, u32[]{:S(2)}) copy-start(bf16[2048,2048]{1,0:T(8,128)(2,1)} %all-gather.2.cloned.1.call-done) | copy-start | bytes 25165828
  123.7 63.2 %copy-start.24 = (bf16[1,2048,512]{2,1,0:T(8,128)(2,1)S(1)}, bf16[1,2048,512]{2,1,0:T(8,128)(2,1)}, u32[]{:S(2)}) copy-start(bf16[1,2048,512]{2,1,0:T(8,128)(2,1)} %param.21) | copy-start | bytes 6291460
  194.2 5.8 %copy-start.22 = (f32[256,2]{0,1:T(2,128)S(1)}, f32[256,2]{0,1:T(2,128)}, u32[]{:S(2)}) copy-start(f32[256,2]{0,1:T(2,128)} %param.25) | copy-start | bytes 6148
  194.2 56.9 %all-to-all-start.2 = ((bf16[64,8,2048]{2,1,0:T(8,128)(2,1)}), bf16[64,8,2048]{2,1,0:T(8,128)(2,1)}, u32[]{:S(2)}, u32[]{:S(2)}) async-start(bf16[64,8,2048]{2,1,0:T(8,128)(2,1)} %fusion.6), calls=%async_computation.2 | async-start | bytes 4194304 | tf_op jit(solution)/shard_map/all_to_all | solution.py:157
  263.7 9.0 %copy-start.3 = (bf16[256,2048]{1,0:T(8,128)(2,1)S(1)}, bf16[256,2048]{1,0:T(8,128)(2,1)}, u32[]{:S(2)}) copy-start(bf16[256,2048]{1,0:T(8,128)(2,1)} %copy-done.2) | copy-start | bytes 3145732
  (12 other events, 25.4 us)
Sparse Core Ops, SparseCore 0:
  9.1 93.9 all-gather.1
where the time goes:
time: 282 us; the launch traced here: 281 us
  waiting for transfers between devices  68.6 us (24%)
  blocking collectives  61.9 us (22%)
  local copies, waits for them, and re-layouts  43.8 us (16%)
  matrix products  33.4 us (12%)
  other arithmetic  32.1 us (11%)
  starting transfers between devices  27 us (10%)
  between operations  13.8 us (5%)
    all_to_all x1, blocking collectives, per_device(): lax.all_to_all(outgoing, 'sp', split_axis=0, concat_axis=0, tiled=True)  61.9 us
    all_to_all x1, waiting for transfers between devices, per_device(): lax.all_to_all(produced.reshape(incoming.shape), 'sp', split_axis=0, conc...  51 us
    all_to_all x1, waiting for transfers between devices, per_device(): lax.all_to_all(attended, 'tp', split_axis=0, concat_axis=1, tiled=True)  16.9 us
    ppermute x3, starting transfers between devices, extended(): lax.ppermute(lax.slice_in_dim(block, 0, width, axis=dim), axis, backward)  10.9 us
    reduce_sum x2, other arithmetic, attend(): jnp.sum(exponent, axis=3, keepdims=True) + jnp.exp(sink_col - row_top)  9.98 us
    dot_general x2, matrix products, attend(): jnp.einsum('qgrd,kgd->grqk', query_heads, key_heads, preferred_element_ty...  9.67 us
    dot_general x2, matrix products, attend(): jnp.einsum('grqk,kgd->qgrd', attn_weight, value_heads, preferred_element_...  9.3 us
    reduce_sum x1, other arithmetic, per_device(): jnp.sum(route_weights[:, :, None] * route_out.astype(jnp.float32), axis=1)  8.96 us
  transfers between devices with their start and end apart: 9, of which 2 were waited for; matrix products, arithmetic and copies ran while one was open for 22% of the time, Pallas kernels for 0%

commit v1 on v0

v1 whole, which is shorter than its diff:
```python
import jax
import jax.numpy as jnp
from jax import lax
from jax.experimental import pallas as pl
from jax.experimental.pallas import tpu as pltpu
from jax.sharding import PartitionSpec as P

HD = 64
BLK = 128
MESH = pl.DeviceIdType.MESH
NEG = -1e30
EPS = 1e-06
BF = jnp.bfloat16
F32 = jnp.float32


def coords():
    s = lax.axis_index("sp")
    y = lax.axis_index("tp")
    c = lax.rem(s, 2)
    x = lax.rem(s // 2, 4)
    z = s // 8
    return s, y, z, x, c


def sp_of(z, x, c):
    return (z * 4 + x) * 2 + c


def front_kernel(
    q_ref, k_ref, v_ref, docs_ref, sink_ref, gain_ref, resid_hbm, w_hbm,
    stream_ref, normed_ref,
    k2, v2, dpad, khalo, vhalo, att, regr, wall, w_own, resid, acc, bias,
    send, recv, lsem,
):
    s, y, z, x, c = coords()
    xm, xp = lax.rem(x + 3, 4), lax.rem(x + 1, 4)
    xo = lax.rem(x + 2, 4)
    sp_next = (lax.rem(s + 1, 64), y)
    sp_prev = (lax.rem(s + 63, 64), y)
    sib = (sp_of(z, x, 1 - c), y)
    x_next = (sp_of(z, xp, c), y)
    x_prev = (sp_of(z, xm, c), y)
    tps = [None] + [(s, lax.rem(y + r, 4)) for r in (1, 2, 3)]

    def rc(src, dst, n, dev):
        return pltpu.make_async_remote_copy(
            src_ref=src, dst_ref=dst, send_sem=send.at[n], recv_sem=recv.at[n],
            device_id=dev, device_id_type=MESH,
        )

    started = []

    def go(src, dst, n, dev):
        d = rc(src, dst, n, dev)
        d.start()
        started.append(d)

    def got(dst, n):
        rc(dst, dst, n, sib).wait_recv()

    w_copy = pltpu.make_async_copy(w_hbm, w_own, lsem.at[0])
    r_copy = pltpu.make_async_copy(resid_hbm, resid, lsem.at[1])
    w_copy.start()
    r_copy.start()
    barrier = pltpu.get_barrier_semaphore()
    for dev in (sp_next, sp_prev, tps[1], tps[2], tps[3], x_next, x_prev):
        pl.semaphore_signal(barrier, inc=1, device_id=dev, device_id_type=MESH)
    pl.semaphore_wait(barrier, 7)

    go(k_ref.at[pl.ds(896, 128)], khalo.at[0], 0, sp_next)
    go(v_ref.at[pl.ds(896, 128)], vhalo.at[0], 1, sp_next)
    go(docs_ref.at[7], dpad.at[0], 2, sp_next)
    go(k_ref.at[pl.ds(0, 128)], khalo.at[1], 3, sp_prev)
    go(v_ref.at[pl.ds(0, 128)], vhalo.at[1], 4, sp_prev)
    go(docs_ref.at[0], dpad.at[9], 5, sp_prev)

    def rows(xx, cc, off, n):
        return pl.ds(pl.multiple_of(128 * xx + 64 * cc + off, 32), n)

    w_copy.wait()
    mine = rows(x, c, 0, 64)
    mine_lo, mine_hi = rows(x, c, 0, 32), rows(x, c, 32, 32)
    go(w_own.at[mine], wall.at[0, mine], 6, tps[1])
    go(w_own.at[mine], wall.at[1, mine], 7, tps[3])

    lane = lax.broadcasted_iota(jnp.int32, (BLK, BLK), 1)
    row = lax.broadcasted_iota(jnp.int32, (BLK, BLK), 0)
    low = lane < 64

    def dup(src, dst, at):
        v = src.astype(F32)
        rolled = pltpu.roll(v, 64, 1)
        dst[0, pl.ds(at, BLK), :] = jnp.where(low, v, rolled).astype(BF)
        dst[1, pl.ds(at, BLK), :] = jnp.where(low, rolled, v).astype(BF)

    @pl.loop(0, 8)
    def _(i):
        at = pl.multiple_of(i * BLK, BLK)
        dup(k_ref[pl.ds(at, BLK), :], k2, at + BLK)
        dup(v_ref[pl.ds(at, BLK), :], v2, at + BLK)
        dpad[i + 1] = docs_ref[i]

    for n, ref in ((0, khalo.at[0]), (1, vhalo.at[0]), (2, dpad.at[0]),
                   (3, khalo.at[1]), (4, vhalo.at[1]), (5, dpad.at[9])):
        got(ref, n)
    dup(khalo[0], k2, 0)
    dup(khalo[1], k2, 9 * BLK)
    dup(vhalo[0], v2, 0)
    dup(vhalo[1], v2, 9 * BLK)
    dpad[0] = jnp.where(s == 0, -1, dpad[0])
    dpad[9] = jnp.where(s == 63, -1, dpad[9])

    scale = HD ** (-0.5)
    mrow = lax.broadcasted_iota(jnp.int32, (BLK, BLK), 1)
    m_even = jnp.where(mrow < 64, scale, 0.0).astype(BF)
    m_odd = jnp.where(mrow < 64, 0.0, scale).astype(BF)

    def pair_of_blocks(t, out, out_at):
        p = lax.rem(y + 1 + t, 4)

        @pl.loop(0, 4)
        def _(it):
            sub = it // 2
            g = lax.rem(it, 2)
            b = 2 * p + sub
            at = pl.multiple_of(b * BLK, BLK)

            @pl.when(g == 0)
            def _():
                qd = jnp.transpose(jnp.broadcast_to(dpad[b + 1].astype(F32), (BLK, BLK)))
                for j in range(3):
                    ok = qd == dpad[b + j].astype(F32)
                    if j == 0:
                        ok = ok & (lane >= row)
                    if j == 2:
                        ok = ok & (lane <= row)
                    bias[:, j * BLK:(j + 1) * BLK] = jnp.where(ok, 0.0, NEG)

            keys = k2[g, pl.ds(at, 3 * BLK), :]
            vals = v2[g, pl.ds(at, 3 * BLK), :]
            for pair in range(2):
                col = pl.multiple_of(g * 256 + pair * BLK, BLK)
                qq = q_ref[pl.ds(at, BLK), pl.ds(col, BLK)]
                outs = []
                for half in range(2):
                    sink = sink_ref[g * 4 + pair * 2 + half]
                    qm = qq * (m_even if half == 0 else m_odd)
                    sc = lax.dot_general(qm, keys, (((1,), (1,)), ((), ())),
                                         preferred_element_type=F32) + bias[...]
                    top = jnp.maximum(jnp.max(sc, axis=1, keepdims=True), sink)
                    ex = jnp.exp(sc - top)
                    den = jnp.sum(ex, axis=1, keepdims=True) + jnp.exp(sink - top)
                    o = jnp.dot(ex.astype(BF), vals, preferred_element_type=F32)
                    outs.append(o * (1.0 / den))
                out[out_at, pl.ds(pl.multiple_of(sub * BLK, BLK), BLK), pl.ds(col, BLK)] = (
                    jnp.where(low, outs[0], outs[1]).astype(BF))

    def send_att(t):
        r = t + 1
        go(att.at[t], regr.at[4 - r], 26 + t, tps[r])

    ab, dd = pl.ds(0, 2), pl.ds(2, 1)
    pair_of_blocks(0, att, 0)
    got(wall.at[0, mine], 6)
    got(wall.at[1, mine], 7)
    go(wall.at[0, mine_lo], wall.at[2, mine_lo], 8, tps[1])
    go(wall.at[1, mine_hi], wall.at[2, mine_hi], 9, tps[3])
    go(wall.at[ab, mine], wall.at[ab, mine], 10, x_next)
    go(wall.at[ab, mine], wall.at[ab, mine], 11, x_prev)
    go(wall.at[ab, mine], wall.at[ab, mine], 18, sib)
    pair_of_blocks(1, att, 1)
    send_att(0)
    pair_of_blocks(2, att, 2)
    send_att(1)
    got(wall.at[2, mine_lo], 8)
    got(wall.at[2, mine_hi], 9)
    go(wall.at[dd, mine], wall.at[dd, mine], 12, x_next)
    go(wall.at[dd, mine], wall.at[dd, mine], 13, x_prev)
    go(wall.at[dd, mine], wall.at[dd, mine], 19, sib)
    pair_of_blocks(3, regr, 0)
    send_att(2)

    from_m, from_p = rows(xm, c, 0, 64), rows(xp, c, 0, 64)
    fm_lo, fp_hi = rows(xm, c, 0, 32), rows(xp, c, 32, 32)
    far, far_lo, far_hi = rows(xo, c, 0, 64), rows(xo, c, 0, 32), rows(xo, c, 32, 32)

    for sh, n, nd in ((ab, 10, 20), (dd, 12, 21)):
        got(wall.at[sh, from_m], n)
        got(wall.at[sh, from_p], n + 1)
        go(wall.at[sh, fm_lo], wall.at[sh, fm_lo], n + 4, x_next)
        go(wall.at[sh, fp_hi], wall.at[sh, fp_hi], n + 5, x_prev)
        go(wall.at[sh, from_m], wall.at[sh, from_m], nd, sib)
        go(wall.at[sh, from_p], wall.at[sh, from_p], nd + 2, sib)

    r_copy.wait()
    acc[...] = resid[...].astype(F32)

    def project(r, wref):
        @pl.loop(0, 4)
        def _(n):
            cols = pl.ds(pl.multiple_of(n * 512, 512), 512)
            part = jnp.dot(regr[r], wref[:, cols], preferred_element_type=F32)
            acc[:, cols] += part.astype(BF).astype(F32)

    project(0, w_own)
    for sh, n, nd in ((ab, 14, 24), (dd, 16, 25)):
        got(wall.at[sh, far_lo], n)
        got(wall.at[sh, far_hi], n + 1)
        go(wall.at[sh, far], wall.at[sh, far], nd, sib)
        for xx, m in ((x, nd - 6), (xm, nd - 4), (xp, nd - 2), (xo, nd)):
            sl = rows(xx, 1 - c, 0, 64)
            got(wall.at[sh, sl], m)
        if n == 14:
            got(regr.at[1], 26 + 2)
            project(1, wall.at[1])
            got(regr.at[3], 26)
            project(3, wall.at[0])
        else:
            got(regr.at[2], 26 + 1)
            project(2, wall.at[2])

    @pl.loop(0, 16)
    def _(i):
        rr = pl.ds(pl.multiple_of(i * 16, 16), 16)
        st = acc[rr, :].astype(BF)
        stream_ref[rr, :] = st
        sf = st.astype(F32)
        sc = lax.rsqrt(jnp.mean(sf * sf, axis=1, keepdims=True) + EPS)
        normed_ref[rr, :] = (sf * sc * gain_ref[...]).astype(BF)

    for d in started:
        d.wait_send()


def front(queries, key_rows, value_rows, doc_ids, sink_logit, residual, out_weight, norm_gain):
    vm = pl.BlockSpec(memory_space=pltpu.VMEM)
    anyspec = pl.BlockSpec(memory_space=pl.ANY)
    return pl.pallas_call(
        front_kernel,
        out_shape=(
            jax.ShapeDtypeStruct((256, 2048), BF),
            jax.ShapeDtypeStruct((256, 2048), BF),
        ),
        in_specs=[vm, vm, vm, vm, pl.BlockSpec(memory_space=pltpu.SMEM), vm, anyspec, anyspec],
        out_specs=(vm, vm),
        scratch_shapes=[
            pltpu.VMEM((2, 1280, 128), BF),
            pltpu.VMEM((2, 1280, 128), BF),
            pltpu.VMEM((10, 1, 128), jnp.int32),
            pltpu.VMEM((2, 128, 128), BF),
            pltpu.VMEM((2, 128, 128), BF),
            pltpu.VMEM((3, 256, 512), BF),
            pltpu.VMEM((4, 256, 512), BF),
            pltpu.VMEM((3, 512, 2048), BF),
            pltpu.VMEM((512, 2048), BF),
            pltpu.VMEM((256, 2048), BF),
            pltpu.VMEM((256, 2048), F32),
            pltpu.VMEM((128, 384), F32),
            pltpu.SemaphoreType.DMA((29,)),
            pltpu.SemaphoreType.DMA((29,)),
            pltpu.SemaphoreType.DMA((2,)),
        ],
        compiler_params=pltpu.CompilerParams(
            collective_id=0, has_side_effects=True, vmem_limit_bytes=60 * 2**20
        ),
        name="front",
    )(
        queries, key_rows, value_rows, doc_ids.reshape(8, 1, 128), sink_logit,
        norm_gain.reshape(1, 2048), residual, out_weight,
    )


def per_device(
    queries,
    key_rows,
    value_rows,
    doc_ids,
    sink_logit,
    residual,
    out_weight,
    norm_gain,
    gate_weight,
    up_weight,
    down_weight,
    routes,
    route_weights,
):
    stream, normed = front(
        queries, key_rows, value_rows, doc_ids, sink_logit, residual, out_weight, norm_gain
    )
    stream_f = stream.astype(jnp.float32)
    home_rows = normed.shape[0]
    width = normed.shape[1]
    route_count = routes.shape[1]
    expert_count = lax.axis_size("sp") * gate_weight.shape[0]
    capacity = route_count * home_rows // expert_count
    flat_routes = routes.reshape(-1)
    one_hot = (flat_routes[:, None] == jnp.arange(expert_count, dtype=jnp.int32)[None, :]).astype(
        jnp.int32
    )
    earlier = jnp.cumsum(one_hot, axis=0) - one_hot
    slot_rank = jnp.sum(earlier * one_hot, axis=1)
    slot_index = flat_routes * capacity + slot_rank
    source_row = (
        jnp.zeros((expert_count * capacity,), jnp.int32)
        .at[slot_index]
        .set(jnp.arange(home_rows * route_count, dtype=jnp.int32) // route_count)
    )
    outgoing = normed[source_row].reshape(expert_count, capacity, width)
    incoming = lax.all_to_all(outgoing, "sp", split_axis=0, concat_axis=0, tiled=True)
    flat_rows = incoming.reshape(-1, width)
    gate_act = jnp.dot(flat_rows, gate_weight[0], preferred_element_type=jnp.float32)
    up_act = jnp.dot(flat_rows, up_weight[0], preferred_element_type=jnp.float32)
    hidden = (jax.nn.silu(gate_act) * up_act).astype(jnp.bfloat16)
    produced = jnp.dot(hidden, down_weight[0], preferred_element_type=jnp.float32).astype(
        jnp.bfloat16
    )
    returned = lax.all_to_all(
        produced.reshape(incoming.shape), "sp", split_axis=0, concat_axis=0, tiled=True
    )
    route_out = returned.reshape(-1, width)[slot_index].reshape(home_rows, route_count, width)
    weighted = jnp.sum(route_weights[:, :, None] * route_out.astype(jnp.float32), axis=1)
    return (stream_f + weighted).astype(jnp.bfloat16)


def solution(mesh):
    return jax.shard_map(
        per_device,
        mesh=mesh,
        in_specs=(
            P("sp", "tp"),
            P("sp", "tp"),
            P("sp", "tp"),
            P("sp"),
            P("tp"),
            P(("sp", "tp"), None),
            P("tp", None),
            P(),
            P("sp", None, None),
            P("sp", None, None),
            P("sp", None, None),
            P(("sp", "tp"), None),
            P(("sp", "tp"), None),
        ),
        out_specs=P(("sp", "tp"), None),
        check_vma=False,
    )
```

time: 282 us -> 214 us (0.76)
  Pallas kernels: 0 us -> 51.2 us
  matrix products: 33.4 us -> 7.24 us
  starting transfers between devices: 27 us -> 5.94 us
  other arithmetic: 32.1 us -> 12.5 us
  local copies, waits for them, and re-layouts: 43.8 us -> 24.8 us
  waiting for transfers between devices: 68.6 us -> 51 us
  between operations: 13.8 us -> 0.14 us
    pallas_call x0 -> x1, Pallas kernels: none -> 51.2 us  [front(): pl.pallas_call(front_kernel, out_shape=(jax.ShapeDtypeStruct((256, 2048),...]
    dot_general x8 -> x0, matrix products: 26.2 us -> none  [the longest x2 9.67 us: attend(): jnp.einsum('qgrd,kgd->grqk', query_heads, key_heads, preferred_element_ty...]
    all_to_all x1 -> x0, waiting for transfers between devices: 16.9 us -> none  [per_device(): lax.all_to_all(attended, 'tp', split_axis=0, concat_axis=1, tiled=True)]
    ppermute x6 -> x0, starting transfers between devices: 16.6 us -> none  [the longest x3 10.9 us: extended(): lax.ppermute(lax.slice_in_dim(block, 0, width, axis=dim), axis, backward)]
    slice x12 -> x1, local copies, waits for them, and re-layouts: 13 us -> 0.23 us  [the longest x2 3.5 us: per_device(): padded_keys[row_start:key_end]]
    reduce_sum x2 -> x0, other arithmetic: 9.98 us -> none  [attend(): jnp.sum(exponent, axis=3, keepdims=True) + jnp.exp(sink_col - row_top)]
    concatenate x4 -> x0, other arithmetic: 5.29 us -> none  [the longest x3 4.25 us: extended(): block = jnp.concatenate([low, block, high], axis=dim)]
    all_to_all x1 -> x0, starting transfers between devices: 4.62 us -> none  [per_device(): lax.all_to_all(attended, 'tp', split_axis=0, concat_axis=1, tiled=True)]
  transfers between devices with their start and end apart: 9 -> 1, of which waited for: 2 -> 1; matrix products, arithmetic and copies ran while one was open for 22% -> 0% of each run, Pallas kernels for 0% -> 0%
where the time goes in v1:
time: 214 us; the launch traced here: 213 us
  blocking collectives  60.5 us (28%)
  Pallas kernels  51.2 us (24%)
  waiting for transfers between devices  51 us (24%)
  local copies, waits for them, and re-layouts  24.8 us (12%)
  other arithmetic  12.5 us (6%)
  matrix products  7.24 us (3%)
  starting transfers between devices  5.94 us (3%)
    all_to_all x1, blocking collectives, per_device(): lax.all_to_all(outgoing, 'sp', split_axis=0, concat_axis=0, tiled=True)  60.5 us
    pallas_call x1, Pallas kernels, front(): pl.pallas_call(front_kernel, out_shape=(jax.ShapeDtypeStruct((256, 2048),...  51.2 us
    all_to_all x1, waiting for transfers between devices, per_device(): lax.all_to_all(produced.reshape(incoming.shape), 'sp', split_axis=0, conc...  51 us
    reduce_sum x1, other arithmetic, per_device(): jnp.sum(route_weights[:, :, None] * route_out.astype(jnp.float32), axis=1)  8.96 us
    gather x1, local copies, waits for them, and re-layouts, per_device(): returned.reshape(-1, width)[slot_index]  7.13 us
    gather x1, local copies, waits for them, and re-layouts, per_device(): outgoing = normed[source_row].reshape(expert_count, capacity, width)  6.65 us
    dot_general x1, matrix products, per_device(): jnp.dot(hidden, down_weight[0], preferred_element_type=jnp.float32)  6 us
    all_to_all x1, starting transfers between devices, per_device(): lax.all_to_all(produced.reshape(incoming.shape), 'sp', split_axis=0, conc...  5.94 us
  transfers between devices with their start and end apart: 1, of which 1 were waited for; matrix products, arithmetic and copies ran while one was open for 0% of the time, Pallas kernels for 0%

profile of v1, /device:TPU:2, one launch (start us, length us, event | category | flops | bytes accessed | tf_op | source)
XLA Modules:
  0.0 213.3 jit_solution(3144781325907895172)
XLA Ops:
  0.0 0.8 broadcast_multiply_fusion
  0.8 0.8 copy.17
  1.7 0.1 eq.29
  1.8 0.1 eq.25
  1.9 0.1 copy.16
  2.1 0.1 mul.37
  2.3 1.2 reduce-window.6
  3.5 0.2 slice_reduce_fusion
  3.7 0.1 fusion.25
  3.9 2.4 %scatter_custom_fusion = s32[512]{0:T(512)S(1)} fusion(s32[512]{0:T(512)S(1)} %bitcast.57, s32[512]{0:T(512)S(1)} %add_select_fusion, s32[]{:T(128)} %constant.25.clone.1), kind=kCustom, calls=%fused_computation.38 | custom fusion | bytes 2052 | tf_op jit(solution)/shard_map/scatter | solution.py:308
  6.3 51.2 %front.1 = (bf16[256,2048]{1,0:T(8,128)(2,1)}, bf16[256,2048]{1,0:T(8,128)(2,1)}) custom-call(bf16[1024,512]{1,0:T(8,128)(2,1)} %q_ref.1, bf16[1024,128]{1,0:T(8,128)(2,1)} %k_ref.1, bf16[1024,128]{1,0:T(8,128)(2,1)} %v_ref.1, s32[8,1,128]{2,1,0:T(1,128)} %bitcast.59, f32[8]{0:T(128)} %sink_ref.1, f32[1,2048]{1,0:T(1,128)} %bitcast.55, ...), custom_call_target="tpu_custom_call" | custom-call | tf_op jit(solution)/shard_map/front/pallas_call | solution.py:239
  57.6 6.6 %gather_fusion = bf16[512,2048]{1,0:T(8,128)(2,1)} fusion(bf16[256,2048]{1,0:T(8,128)(2,1)} %get-tuple-element.8, s32[1024]{0:T(1024)S(1)} %pad_clamp_fusion.1), kind=kCustom, calls=%fused_computation | custom fusion | bytes 4196352 | tf_op jit(solution)/shard_map/gather | solution.py:310
  64.3 60.5 %all_to_all.10 = bf16[64,8,2048]{2,1,0:T(8,128)(2,1)S(1)} all-to-all(bf16[64,8,2048]{2,1,0:T(8,128)(2,1)} %bitcast.54), channel_id=1, replica_groups=mesh['sp'=64,'tp'=4] {'sp'}, dimensions={0} | all-to-all | bytes 4194304 | tf_op jit(solution)/shard_map/all_to_all | solution.py:311
  124.7 1.3 copy-done.1
  126.1 1.2 fusion.4
  127.3 0.0 copy-done
  127.3 6.0 %fusion = bf16[64,8,2048]{2,1,0:T(8,128)(2,1)} fusion(bf16[1,512,2048]{2,1,0:T(8,128)(2,1)S(1)} %copy-done, bf16[1,2048,512]{2,1,0:T(8,128)(2,1)} %param.22, bf16[64,8,2048]{2,1,0:T(8,128)(2,1)} %copy-done.1, f32[512,512]{1,0:T(8,128)S(1)} %fusion.4), kind=kOutput, calls=%fused_computation.5 | convolution fusion | flops 2150105088 | bytes 9437184 | tf_op jit(solution)/shard_map/dot_general | solution.py:316
  133.3 5.9 %all-to-all-start.1 = ((bf16[64,8,2048]{2,1,0:T(8,128)(2,1)}), bf16[64,8,2048]{2,1,0:T(8,128)(2,1)}, u32[]{:S(2)}, u32[]{:S(2)}) async-start(bf16[64,8,2048]{2,1,0:T(8,128)(2,1)} %fusion), calls=%async_computation.1 | async-start | bytes 4194304 | tf_op jit(solution)/shard_map/all_to_all | solution.py:319
  139.3 0.1 copy.15
  139.5 51.0 %all-to-all-done.1 = bf16[64,8,2048]{2,1,0:T(8,128)(2,1)} async-done(((bf16[64,8,2048]{2,1,0:T(8,128)(2,1)}), bf16[64,8,2048]{2,1,0:T(8,128)(2,1)}, u32[]{:S(2)}, u32[]{:S(2)}) %all-to-all-start.1) | async-done | bytes 2097184 | tf_op jit(solution)/shard_map/all_to_all | solution.py:319
  190.4 7.1 %gather_fusion.1 = bf16[512,2048]{1,0:T(8,128)(2,1)} fusion(bf16[512,2048]{1,0:T(8,128)(2,1)} %bitcast.11, s32[1024]{0:T(1024)S(1)} %pad_clamp_fusion), kind=kCustom, calls=%fused_computation.1 | custom fusion | bytes 4196352 | tf_op jit(solution)/shard_map/gather | solution.py:322
  197.6 5.4 %reshape.75 = f32[256,2,2048]{2,1,0:T(2,128)} reshape(bf16[512,2048]{1,0:T(8,128)(2,1)} %gather_fusion.1) | data formatting | bytes 6291456 | tf_op jit(solution)/shard_map/convert_element_type | solution.py:323
  203.0 9.0 %multiply_reduce_fusion = f32[256,2048]{1,0:T(8,128)S(1)} fusion(f32[256,2,2048]{2,1,0:T(2,128)} %reshape.75, f32[256,2]{1,0:T(8,128)S(1)} %copy.15), kind=kLoop, calls=%fused_computation.3 | loop fusion | flops 1572864 | bytes 6293504 | tf_op jit(solution)/shard_map/reduce_sum | solution.py:323
  212.0 1.3 add_convert_fusion
  (16 shorter events, 0.1 us)
Async XLA Ops:
  0.0 127.3 %copy-start = (bf16[1,512,2048]{2,1,0:T(8,128)(2,1)S(1)}, bf16[1,512,2048]{2,1,0:T(8,128)(2,1)}, u32[]{:S(2)}) copy-start(bf16[1,512,2048]{2,1,0:T(8,128)(2,1)} %param.23) | copy-start | bytes 6291460
  64.3 61.8 %copy-start.4 = (bf16[1,2048,512]{2,1,0:T(8,128)(2,1)S(1)}, bf16[1,2048,512]{2,1,0:T(8,128)(2,1)}, u32[]{:S(2)}) copy-start(bf16[1,2048,512]{2,1,0:T(8,128)(2,1)} %param.21) | copy-start | bytes 6291460
  124.7 1.4 copy-start.1
  133.3 6.0 %copy-start.3 = (f32[256,2]{0,1:T(2,128)S(1)}, f32[256,2]{0,1:T(2,128)}, u32[]{:S(2)}) copy-start(f32[256,2]{0,1:T(2,128)} %param.25) | copy-start | bytes 6148
  133.3 57.1 %all-to-all-start.1 = ((bf16[64,8,2048]{2,1,0:T(8,128)(2,1)}), bf16[64,8,2048]{2,1,0:T(8,128)(2,1)}, u32[]{:S(2)}, u32[]{:S(2)}) async-start(bf16[64,8,2048]{2,1,0:T(8,128)(2,1)} %fusion), calls=%async_computation.1 | async-start | bytes 4194304 | tf_op jit(solution)/shard_map/all_to_all | solution.py:319
  203.0 9.0 %copy-start.2 = (bf16[256,2048]{1,0:T(8,128)(2,1)S(1)}, bf16[256,2048]{1,0:T(8,128)(2,1)}, u32[]{:S(2)}) copy-start(bf16[256,2048]{1,0:T(8,128)(2,1)} %get-tuple-element.7) | copy-start | bytes 3145732

commit v2 on v1

--- a/solution.py
+++ b/solution.py
@@ -271,6 +271,290 @@
     )
 
 
+PAIRS = ((0, 4), (1, 2), (3, 5), (6, 7))
+
+
+def moe_kernel(
+    normed_ref, stream_ref, routes_ref, rw_ref, gate_hbm, up_hbm, down_hbm,
+    mixed_ref,
+    sbuf, land, metas, metar, mscr, pg_t, whi, wlo, xbuf, xin, pbuf, rbuf,
+    partk, psend, cback, totb, fin, wg, wu, wd, send, recv, lsem,
+):
+    s, y, z, x, c = coords()
+    me = 2 * x + c
+    zl = lax.rem(z, 2)
+    g_me = z // 2
+    sgn = 2 * zl - 1
+
+    def zdev(zz):
+        return (sp_of(lax.rem(zz + 16, 8), x, c), y)
+
+    def xdev(i):
+        i = lax.rem(i + 8, 8)
+        return (sp_of(z, i // 2, lax.rem(i, 2)), y)
+
+    partner = zdev(z - sgn)
+
+    def rc(src, dst, n, dev):
+        return pltpu.make_async_remote_copy(
+            src_ref=src, dst_ref=dst, send_sem=send.at[n], recv_sem=recv.at[n],
+            device_id=dev, device_id_type=MESH,
+        )
+
+    pending = []
+
+    def go(src, dst, n, dev, note=True):
+        d = rc(src, dst, n, dev)
+        d.start()
+        if note:
+            pending.append(d)
+
+    def got(dst, n):
+        rc(dst, dst, n, partner).wait_recv()
+
+    loads = [pltpu.make_async_copy(a, b, lsem.at[i])
+             for i, (a, b) in enumerate(((gate_hbm.at[0], wg), (up_hbm.at[0], wu), (down_hbm.at[0], wd)))]
+    for cp in loads:
+        cp.start()
+    barrier = pltpu.get_barrier_semaphore()
+    for o in range(1, 8):
+        pl.semaphore_signal(barrier, inc=1, device_id=zdev(z + o), device_id_type=MESH)
+        pl.semaphore_signal(barrier, inc=1, device_id=xdev(me + o), device_id_type=MESH)
+
+    e0, e1 = routes_ref[0:1, :], routes_ref[1:2, :]
+    upper = (lax.broadcasted_iota(jnp.int32, (256, 256), 0)
+             < lax.broadcasted_iota(jnp.int32, (256, 256), 1)).astype(F32).astype(BF)
+    ei = lax.broadcasted_iota(jnp.int32, (64, 256), 0)
+    h0 = (ei == e0).astype(F32)
+    h1 = (ei == e1).astype(F32)
+    hg = (lax.broadcasted_iota(jnp.int32, (16, 256), 0) == (e0 >> 4)).astype(F32)
+
+    def before(h):
+        return jnp.dot(h.astype(BF), upper, preferred_element_type=F32)
+
+    rank0 = jnp.sum(h0 * before(h0), axis=0, keepdims=True)
+    rank1 = jnp.sum(h1 * (before(h1) + jnp.sum(h0, axis=1, keepdims=True)), axis=0, keepdims=True)
+    gpos = jnp.sum(hg * before(hg), axis=0, keepdims=True) + ((e0 >> 4) * 64).astype(F32)
+    w0, w1 = rw_ref[0:1, :], rw_ref[1:2, :]
+    w0h = w0.astype(BF).astype(F32)
+    w1h = w1.astype(BF).astype(F32)
+    mscr[...] = jnp.zeros((16, 256), F32)
+    mscr[0:1, :] = ((e0 & 15) * 8).astype(F32) + rank0
+    mscr[1:2, :] = ((e1 & 15) * 8).astype(F32) + rank1
+    mscr[2:3, :] = w0h
+    mscr[3:4, :] = w0 - w0h
+    mscr[4:5, :] = w1h
+    mscr[5:6, :] = w1 - w1h
+    pg = (lax.broadcasted_iota(jnp.int32, (256, 256), 0).astype(F32) == gpos).astype(F32)
+    pg_t[...] = jnp.transpose(pg).astype(BF)
+    pgb = pg.astype(BF)
+    info = mscr[...].astype(BF)
+    for g in range(4):
+        pgg = pgb[64 * g:64 * (g + 1), :]
+        both = jnp.concatenate([pgg, pgg], axis=0)
+        metas[g] = lax.dot_general(info, both, (((1,), (1,)), ((), ())),
+                                   preferred_element_type=F32)[0:8, :]
+
+    @pl.loop(0, 8)
+    def _(n):
+        cols = pl.ds(pl.multiple_of(n * 256, 256), 256)
+        out = jnp.dot(pgb, normed_ref[:, cols], preferred_element_type=F32).astype(BF)
+        for g in range(4):
+            sbuf[g, :, cols] = out[64 * g:64 * (g + 1), :]
+
+    pl.semaphore_wait(barrier, 14)
+
+    g_of = [g_me, lax.rem(g_me + sgn + 4, 4), lax.rem(g_me - sgn + 4, 4), lax.rem(g_me + 2, 4)]
+    t_of = [None, z + sgn, z - 2 * sgn, z + 3 * sgn]
+    for o in range(1, 8):
+        zz = lax.rem(z + o, 8)
+        go(metas.at[zz // 2], metar.at[o], o, zdev(z + o))
+    metar[0] = metas[g_me]
+    go(sbuf.at[g_of[1]], land.at[1], 9, zdev(t_of[1]))
+    go(sbuf.at[g_me], land.at[4], 8, partner)
+    go(sbuf.at[g_of[3]], land.at[3], 11, zdev(t_of[3]))
+    go(sbuf.at[g_of[2]], land.at[2], 10, zdev(t_of[2]))
+    for o in range(1, 8):
+        got(metar.at[o], o)
+
+    def origin(b):
+        if b == 0:
+            return 0
+        if b < 4:
+            return lax.rem(8 - sgn * b, 8)
+        return lax.rem(8 + sgn * (b - 3), 8)
+
+    def fwd(k):
+        got(land.at[k], 8 + k)
+        go(land.at[k], land.at[4 + k], 11 + k, partner)
+
+    lane = lax.broadcasted_iota(jnp.int32, (128, 128), 1)
+    ii = lax.broadcasted_iota(jnp.int32, (128, 128), 0)
+
+    def exchange(p):
+        b0, b1 = PAIRS[p]
+        mm = jnp.where(lane[0:8, :] < 64, metar[origin(b0)], metar[origin(b1)])
+        slot = ((((ii >> 4) + me) & 7) << 3) + (ii & 7) + 64 * zl
+        slot = jnp.where(((ii >> 3) & 1) == (lane >> 6), slot, -1).astype(F32)
+        hit0 = slot == mm[0:1, :]
+        hit1 = slot == mm[1:2, :]
+        sel = jnp.where(hit0 | hit1, 1.0, 0.0).astype(BF)
+        for r, ref in ((2, whi), (3, wlo)):
+            wt = jnp.where(hit0, mm[r:r + 1, :], 0.0) + jnp.where(hit1, mm[r + 2:r + 3, :], 0.0)
+            ref[p] = jnp.transpose(wt).astype(BF)
+        first = sbuf.at[g_me] if b0 == 0 else land.at[b0]
+
+        @pl.loop(0, 4)
+        def _(n):
+            cols = pl.ds(pl.multiple_of(n * 512, 512), 512)
+            rows = jnp.concatenate([first[:, cols], land[b1, :, cols]], axis=0)
+            out = jnp.dot(sel, rows, preferred_element_type=F32).astype(BF)
+            xbuf[p, :, cols] = out
+            xin[p, 0:16, cols] = out[0:16, :]
+
+        for o in (2, 6, 4, 5, 3, 7, 1):
+            sl = pl.ds(16 * o, 16)
+            go(xbuf.at[p, sl], xin.at[p, sl], 15 + p, xdev(me + o), note=False)
+
+    rest = pl.ds(16, 112)
+
+    def expert(p):
+        got(xin.at[p, rest], 15 + p)
+        rows = xin[p]
+        gate_act = jnp.dot(rows, wg[...], preferred_element_type=F32)
+        up_act = jnp.dot(rows, wu[...], preferred_element_type=F32)
+        hidden = (gate_act / (1.0 + jnp.exp(-gate_act)) * up_act).astype(BF)
+
+        @pl.loop(0, 4)
+        def _(n):
+            cols = pl.ds(pl.multiple_of(n * 512, 512), 512)
+            out = jnp.dot(hidden, wd[:, cols], preferred_element_type=F32).astype(BF)
+            pbuf[p, :, cols] = out
+            rbuf[p, 0:16, cols] = out[0:16, :]
+
+        for o in (2, 6, 4, 5, 3, 7, 1):
+            sl = pl.ds(16 * o, 16)
+            go(pbuf.at[p, sl], rbuf.at[p, sl], 19 + p, xdev(me - o), note=False)
+
+    def merge(p):
+        got(rbuf.at[p, rest], 19 + p)
+
+        @pl.loop(0, 4)
+        def _(n):
+            cols = pl.ds(pl.multiple_of(n * 512, 512), 512)
+            rows = rbuf[p, :, cols]
+            out = (jnp.dot(whi[p], rows, preferred_element_type=F32)
+                   + jnp.dot(wlo[p], rows, preferred_element_type=F32))
+            for h, b in enumerate(PAIRS[p]):
+                piece = out[64 * h:64 * (h + 1), :]
+                if b < 4:
+                    partk[b, :, cols] = piece
+                else:
+                    psend[b - 4, :, cols] = piece.astype(BF)
+
+        for b in PAIRS[p]:
+            if b >= 4:
+                go(psend.at[b - 4], cback.at[b - 4], 19 + b, partner)
+
+    def total(j):
+        got(cback.at[j], 23 + j)
+
+        @pl.loop(0, 4)
+        def _(n):
+            cols = pl.ds(pl.multiple_of(n * 512, 512), 512)
+            out = (partk[j, :, cols] + cback[j, :, cols].astype(F32)).astype(BF)
+            if j == 0:
+                fin[g_me, :, cols] = out
+            else:
+                totb[j - 1, :, cols] = out
+
+        if j:
+            go(totb.at[j - 1], fin.at[g_me], 26 + j, zdev(z + sgn * j))
+
+    fwd(1)
+    got(land.at[4], 8)
+    exchange(0)
+    fwd(2)
+    exchange(1)
+    for cp in loads:
+        cp.wait()
+    expert(0)
+    fwd(3)
+    got(land.at[5], 12)
+    exchange(2)
+    expert(1)
+    merge(0)
+    expert(2)
+    merge(1)
+    got(land.at[6], 13)
+    got(land.at[7], 14)
+    exchange(3)
+    merge(2)
+    total(0)
+    expert(3)
+    total(1)
+    merge(3)
+    total(2)
+    total(3)
+    for k in (1, 2, 3):
+        got(fin.at[g_of[k]], 26 + k)
+
+    @pl.loop(0, 8)
+    def _(n):
+        cols = pl.ds(pl.multiple_of(n * 256, 256), 256)
+        out = stream_ref[:, cols].astype(F32)
+        rows = jnp.concatenate([fin[g, :, cols] for g in range(4)], axis=0)
+        out += jnp.dot(pg_t[...], rows, preferred_element_type=F32)
+        mixed_ref[:, cols] = out.astype(BF)
+
+    for d in pending:
+        d.wait_send()
+    for p in range(4):
+        rc(xbuf.at[p, rest], xbuf.at[p, rest], 15 + p, partner).wait_send()
+        rc(pbuf.at[p, rest], pbuf.at[p, rest], 19 + p, partner).wait_send()
+
+
+def moe(normed, stream, routes, route_weights, gate_weight, up_weight, down_weight):
+    vm = pl.BlockSpec(memory_space=pltpu.VMEM)
+    anyspec = pl.BlockSpec(memory_space=pl.ANY)
+    big = (4, 128, 2048)
+    return pl.pallas_call(
+        moe_kernel,
+        out_shape=jax.ShapeDtypeStruct((256, 2048), BF),
+        in_specs=[vm, vm, vm, vm, anyspec, anyspec, anyspec],
+        out_specs=vm,
+        scratch_shapes=[
+            pltpu.VMEM((4, 64, 2048), BF),
+            pltpu.VMEM((8, 64, 2048), BF),
+            pltpu.VMEM((4, 8, 128), F32),
+            pltpu.VMEM((8, 8, 128), F32),
+            pltpu.VMEM((16, 256), F32),
+            pltpu.VMEM((256, 256), BF),
+            pltpu.VMEM((4, 128, 128), BF),
+            pltpu.VMEM((4, 128, 128), BF),
+            pltpu.VMEM(big, BF),
+            pltpu.VMEM(big, BF),
+            pltpu.VMEM(big, BF),
+            pltpu.VMEM(big, BF),
+            pltpu.VMEM((4, 64, 2048), F32),
+            pltpu.VMEM((4, 64, 2048), BF),
+            pltpu.VMEM((4, 64, 2048), BF),
+            pltpu.VMEM((3, 64, 2048), BF),
+            pltpu.VMEM((4, 64, 2048), BF),
+            pltpu.VMEM((2048, 512), BF),
+            pltpu.VMEM((2048, 512), BF),
+            pltpu.VMEM((512, 2048), BF),
+            pltpu.SemaphoreType.DMA((30,)),
+            pltpu.SemaphoreType.DMA((30,)),
+            pltpu.SemaphoreType.DMA((3,)),
+        ],
+        compiler_params=pltpu.CompilerParams(
+            collective_id=1, has_side_effects=True, vmem_limit_bytes=60 * 2**20
+        ),
+        name="moe",
+    )(normed, stream, routes.T, route_weights.T, gate_weight, up_weight, down_weight)
+
+
 def per_device(
     queries,
     key_rows,
@@ -289,39 +573,7 @@
     stream, normed = front(
         queries, key_rows, value_rows, doc_ids, sink_logit, residual, out_weight, norm_gain
     )
-    stream_f = stream.astype(jnp.float32)
-    home_rows = normed.shape[0]
-    width = normed.shape[1]
-    route_count = routes.shape[1]
-    expert_count = lax.axis_size("sp") * gate_weight.shape[0]
-    capacity = route_count * home_rows // expert_count
-    flat_routes = routes.reshape(-1)
-    one_hot = (flat_routes[:, None] == jnp.arange(expert_count, dtype=jnp.int32)[None, :]).astype(
-        jnp.int32
-    )
-    earlier = jnp.cumsum(one_hot, axis=0) - one_hot
-    slot_rank = jnp.sum(earlier * one_hot, axis=1)
-    slot_index = flat_routes * capacity + slot_rank
-    source_row = (
-        jnp.zeros((expert_count * capacity,), jnp.int32)
-        .at[slot_index]
-        .set(jnp.arange(home_rows * route_count, dtype=jnp.int32) // route_count)
-    )
-    outgoing = normed[source_row].reshape(expert_count, capacity, width)
-    incoming = lax.all_to_all(outgoing, "sp", split_axis=0, concat_axis=0, tiled=True)
-    flat_rows = incoming.reshape(-1, width)
-    gate_act = jnp.dot(flat_rows, gate_weight[0], preferred_element_type=jnp.float32)
-    up_act = jnp.dot(flat_rows, up_weight[0], preferred_element_type=jnp.float32)
-    hidden = (jax.nn.silu(gate_act) * up_act).astype(jnp.bfloat16)
-    produced = jnp.dot(hidden, down_weight[0], preferred_element_type=jnp.float32).astype(
-        jnp.bfloat16
-    )
-    returned = lax.all_to_all(
-        produced.reshape(incoming.shape), "sp", split_axis=0, concat_axis=0, tiled=True
-    )
-    route_out = returned.reshape(-1, width)[slot_index].reshape(home_rows, route_count, width)
-    weighted = jnp.sum(route_weights[:, :, None] * route_out.astype(jnp.float32), axis=1)
-    return (stream_f + weighted).astype(jnp.bfloat16)
+    return moe(normed, stream, routes, route_weights, gate_weight, up_weight, down_weight)
 
 
 def solution(mesh):

time: 214 us -> 163 us (0.76)
  Pallas kernels: 51.2 us -> 159 us
  blocking collectives: 60.5 us -> 0 us
  waiting for transfers between devices: 51 us -> 0 us
  local copies, waits for them, and re-layouts: 24.8 us -> 2.3 us
  other arithmetic: 12.5 us -> 0 us
  matrix products: 7.24 us -> 0 us
  starting transfers between devices: 5.94 us -> 0 us
    pallas_call x0 -> x1, Pallas kernels: none -> 107 us  [moe(): pl.pallas_call(moe_kernel, out_shape=jax.ShapeDtypeStruct((256, 2048), BF...]
    all_to_all x1 -> x0, blocking collectives: 60.5 us -> none  [per_device(): lax.all_to_all(outgoing, 'sp', split_axis=0, concat_axis=0, tiled=True)]
    all_to_all x1 -> x0, waiting for transfers between devices: 51 us -> none  [per_device(): lax.all_to_all(produced.reshape(incoming.shape), 'sp', split_axis=0, conc...]
    gather x2 -> x0, local copies, waits for them, and re-layouts: 13.8 us -> none  [the longest x1 7.13 us: per_device(): returned.reshape(-1, width)[slot_index]]
    reduce_sum x2 -> x0, other arithmetic: 9.09 us -> none  [the longest x1 8.96 us: per_device(): jnp.sum(route_weights[:, :, None] * route_out.astype(jnp.float32), axis=1)]
    dot_general x2 -> x0, matrix products: 7.24 us -> none  [the longest x1 6 us: per_device(): jnp.dot(hidden, down_weight[0], preferred_element_type=jnp.float32)]
    all_to_all x1 -> x0, starting transfers between devices: 5.94 us -> none  [per_device(): lax.all_to_all(produced.reshape(incoming.shape), 'sp', split_axis=0, conc...]
    convert_element_type x1 -> x0, local copies, waits for them, and re-layouts: 5.44 us -> none  [per_device(): route_out.astype(jnp.float32)]
  transfers between devices with their start and end apart: 1 -> 0, of which waited for: 1 -> 0; matrix products, arithmetic and copies ran while one was open for 0% -> 0% of each run, Pallas kernels for 0% -> 0%
where the time goes in v2:
time: 163 us; the launch traced here: 161 us
  Pallas kernels  159 us (98%)
  local copies, waits for them, and re-layouts  2.3 us (1%)
    pallas_call x1, Pallas kernels, moe(): pl.pallas_call(moe_kernel, out_shape=jax.ShapeDtypeStruct((256, 2048), BF...  107 us
    pallas_call x1, Pallas kernels, front(): pl.pallas_call(front_kernel, out_shape=(jax.ShapeDtypeStruct((256, 2048),...  51.2 us

profile of v2, /device:TPU:2, one launch (start us, length us, event | category | flops | bytes accessed | tf_op | source)
XLA Modules:
  0.0 160.9 jit_solution(11841702550732923420)
XLA Ops:
  0.0 51.2 %front.1 = (bf16[256,2048]{1,0:T(8,128)(2,1)}, bf16[256,2048]{1,0:T(8,128)(2,1)}) custom-call(bf16[1024,512]{1,0:T(8,128)(2,1)} %q_ref.1, bf16[1024,128]{1,0:T(8,128)(2,1)} %k_ref.1, bf16[1024,128]{1,0:T(8,128)(2,1)} %v_ref.1, s32[8,1,128]{2,1,0:T(1,128)} %bitcast.5, f32[8]{0:T(128)} %sink_ref.1, f32[1,2048]{1,0:T(1,128)} %bitcast.4, ...), custom_call_target="tpu_custom_call" | custom-call | tf_op jit(solution)/shard_map/front/pallas_call | solution.py:239
  51.2 107.5 %moe.1 = bf16[256,2048]{1,0:T(8,128)(2,1)} custom-call(bf16[256,2048]{1,0:T(8,128)(2,1)} %get-tuple-element.7.normed_ref, bf16[256,2048]{1,0:T(8,128)(2,1)} %get-tuple-element.8.stream_ref, s32[2,256]{1,0:T(2,128)} %bitcast.6, f32[2,256]{1,0:T(2,128)} %bitcast.7, bf16[1,2048,512]{2,1,0:T(8,128)(2,1)} %gate_hbm.1, bf16[1,2048,512]{2,1,0:T(8,128)(2,1)} %up_hbm.1, ...), custom_call_target="tpu_custom_call" | custom-call | tf_op jit(solution)/shard_map/moe/pallas_call | solution.py:521
  158.6 2.3 %copy.15 = bf16[256,2048]{1,0:T(8,128)(2,1)} copy(bf16[256,2048]{1,0:T(8,128)(2,1)} %moe.1) | data formatting | bytes 2097152

commit v3 on v1

v3 whole, which is shorter than its diff:
```python
import jax
import jax.numpy as jnp
from jax import lax
from jax.experimental import pallas as pl
from jax.experimental.pallas import tpu as pltpu
from jax.sharding import PartitionSpec as P

HD = 64
BLK = 128
MESH = pl.DeviceIdType.MESH
NEG = -1e30
EPS = 1e-06
BF = jnp.bfloat16
F32 = jnp.float32


def coords():
    s = lax.axis_index("sp")
    y = lax.axis_index("tp")
    c = lax.rem(s, 2)
    x = lax.rem(s // 2, 4)
    z = s // 8
    return s, y, z, x, c


def sp_of(z, x, c):
    return (z * 4 + x) * 2 + c


PAIRS = ((0, 1), (2, 3), (5, 6), (7, 4))


def layer_kernel(
    q_ref, k_ref, v_ref, docs_ref, sink_ref, gain_ref, routes_ref, rw_ref,
    resid_hbm, w_hbm, gate_hbm, up_hbm, down_hbm,
    mixed_ref,
    k2, v3, dpad, khalo, vhalo, att, regr, wall, w_own, resid, acc, bias, scores, probs, squares,
    stream, sbuf, land, metas, metar, mscr, pg_n, pg_t, whi, wlo, xbuf, xin, pbuf, rbuf,
    partk, psend, cback, totb, fin, wg, wu, wd, fsend, frecv, msend, mrecv, lsem,
):
    s, y, z, x, c = coords()
    xm, xp = lax.rem(x + 3, 4), lax.rem(x + 1, 4)
    xo = lax.rem(x + 2, 4)
    me = 2 * x + c
    zl = lax.rem(z, 2)
    g_me = z // 2
    sgn = 2 * zl - 1

    def zdev(zz):
        return (sp_of(lax.rem(zz + 16, 8), x, c), y)

    def xdev(i):
        i = lax.rem(i + 8, 8)
        return (sp_of(z, i // 2, lax.rem(i, 2)), y)

    sp_next = (lax.rem(s + 1, 64), y)
    sp_prev = (lax.rem(s + 63, 64), y)
    sib = (sp_of(z, x, 1 - c), y)
    x_next = (sp_of(z, xp, c), y)
    x_prev = (sp_of(z, xm, c), y)
    z_next, z_prev = zdev(z + 1), zdev(z - 1)
    tps = [None] + [(s, lax.rem(y + r, 4)) for r in (1, 2, 3)]
    partner = zdev(z - sgn)

    def rc(src, dst, n, dev):
        return pltpu.make_async_remote_copy(
            src_ref=src, dst_ref=dst, send_sem=fsend.at[n], recv_sem=frecv.at[n],
            device_id=dev, device_id_type=MESH,
        )

    pending = []

    def go(src, dst, n, dev):
        d = rc(src, dst, n, dev)
        d.start()
        pending.append(d)

    def got(dst, n):
        rc(dst, dst, n, sib).wait_recv()


    def mrc(src, dst, n, dev):
        return pltpu.make_async_remote_copy(
            src_ref=src, dst_ref=dst, send_sem=msend.at[n], recv_sem=mrecv.at[n],
            device_id=dev, device_id_type=MESH,
        )

    def mgo(src, dst, n, dev, note=True):
        d = mrc(src, dst, n, dev)
        d.start()
        if note:
            pending.append(d)

    def mgot(dst, n):
        mrc(dst, dst, n, partner).wait_recv()

    w_copy = pltpu.make_async_copy(w_hbm, w_own, lsem.at[0])
    r_copy = pltpu.make_async_copy(resid_hbm, resid, lsem.at[1])
    w_copy.start()
    r_copy.start()
    loads = [pltpu.make_async_copy(a, b, lsem.at[2 + i])
             for i, (a, b) in enumerate(((gate_hbm.at[0], wg), (up_hbm.at[0], wu), (down_hbm.at[0], wd)))]
    for cp in loads:
        cp.start()
    barrier = pltpu.get_barrier_semaphore()
    greet = [sp_next, sp_prev, tps[1], tps[2], tps[3]]
    greet += [zdev(z + o) for o in range(1, 8)] + [xdev(me + o) for o in range(1, 8)]
    for dev in greet:
        pl.semaphore_signal(barrier, inc=1, device_id=dev, device_id_type=MESH)
    pl.semaphore_wait(barrier, len(greet))

    go(k_ref.at[pl.ds(896, 128)], khalo.at[0], 0, sp_next)
    go(v_ref.at[pl.ds(896, 128)], vhalo.at[0], 1, sp_next)
    go(docs_ref.at[7], dpad.at[0], 2, sp_next)
    go(k_ref.at[pl.ds(0, 128)], khalo.at[1], 3, sp_prev)
    go(v_ref.at[pl.ds(0, 128)], vhalo.at[1], 4, sp_prev)
    go(docs_ref.at[0], dpad.at[9], 5, sp_prev)

    def rows_a(xx, cc, off, n):
        return pl.ds(pl.multiple_of(64 * xx + 32 * cc + off, 16), n)

    def rows_b(zz, cc):
        return pl.ds(pl.multiple_of(256 + 32 * lax.rem(zz + 16, 8) + 16 * cc, 16), 16)

    left, right = pl.ds(0, 1024), pl.ds(1024, 1024)
    w_copy.wait()
    mine = rows_a(x, c, 0, 32)
    mine_lo, mine_hi = rows_a(x, c, 0, 16), rows_a(x, c, 16, 16)
    mine_b = rows_b(z, c)
    go(w_own.at[mine], wall.at[0, mine], 6, tps[1])
    go(w_own.at[mine], wall.at[1, mine], 7, tps[3])
    go(w_own.at[mine_b], wall.at[0, mine_b], 30, tps[1])
    go(w_own.at[mine_b], wall.at[1, mine_b], 31, tps[3])

    e0, e1 = routes_ref[0:1, :], routes_ref[1:2, :]
    upper = (lax.broadcasted_iota(jnp.int32, (256, 256), 0)
             < lax.broadcasted_iota(jnp.int32, (256, 256), 1)).astype(F32).astype(BF)
    ei = lax.broadcasted_iota(jnp.int32, (64, 256), 0)
    h0 = (ei == e0).astype(F32)
    h1 = (ei == e1).astype(F32)
    hg = (lax.broadcasted_iota(jnp.int32, (16, 256), 0) == (e0 >> 4)).astype(F32)

    def before(h):
        return jnp.dot(h.astype(BF), upper, preferred_element_type=F32)

    rank0 = jnp.sum(h0 * before(h0), axis=0, keepdims=True)
    rank1 = jnp.sum(h1 * (before(h1) + jnp.sum(h0, axis=1, keepdims=True)), axis=0, keepdims=True)
    gpos = jnp.sum(hg * before(hg), axis=0, keepdims=True) + ((e0 >> 4) * 64).astype(F32)
    w0, w1 = rw_ref[0:1, :], rw_ref[1:2, :]
    w0h = w0.astype(BF).astype(F32)
    w1h = w1.astype(BF).astype(F32)
    mscr[...] = jnp.zeros((16, 256), F32)
    mscr[0:1, :] = ((e0 & 15) * 8).astype(F32) + rank0
    mscr[1:2, :] = ((e1 & 15) * 8).astype(F32) + rank1
    mscr[2:3, :] = w0h
    mscr[3:4, :] = w0 - w0h
    mscr[4:5, :] = w1h
    mscr[5:6, :] = w1 - w1h
    pg = (lax.broadcasted_iota(jnp.int32, (256, 256), 0).astype(F32) == gpos).astype(F32)
    pg_t[...] = jnp.transpose(pg).astype(BF)
    pgb = pg.astype(BF)
    pg_n[...] = pgb
    info = mscr[...].astype(BF)
    for g in range(4):
        pgg = pgb[64 * g:64 * (g + 1), :]
        both = jnp.concatenate([pgg, pgg], axis=0)
        metas[g] = lax.dot_general(info, both, (((1,), (1,)), ((), ())),
                                   preferred_element_type=F32)[0:8, :]

    for o in range(1, 8):
        zz = lax.rem(z + o, 8)
        mgo(metas.at[zz // 2], metar.at[o], o, zdev(z + o))
    metar[0] = metas[g_me]

    lane = lax.broadcasted_iota(jnp.int32, (BLK, BLK), 1)
    row = lax.broadcasted_iota(jnp.int32, (BLK, BLK), 0)
    low = lane < 64

    def dup(src, dst, at):
        v = src.astype(F32)
        rolled = pltpu.roll(v, 64, 1)
        dst[0, pl.ds(at, BLK), 0:BLK] = jnp.where(low, v, rolled).astype(BF)
        dst[1, pl.ds(at, BLK), 0:BLK] = jnp.where(low, rolled, v).astype(BF)

    @pl.loop(0, 8)
    def _(i):
        at = pl.multiple_of(i * BLK, BLK)
        dup(k_ref[pl.ds(at, BLK), :], k2, at + BLK)
        dup(v_ref[pl.ds(at, BLK), :], v3, at + BLK)
        dpad[i + 1] = docs_ref[i]

    @pl.loop(0, 10)
    def _(i):
        at = pl.multiple_of(i * BLK, BLK)
        for g in range(2):
            v3[g, pl.ds(at, BLK), BLK:2 * BLK] = jnp.ones((BLK, BLK), BF)

    for n, ref in ((0, khalo.at[0]), (1, vhalo.at[0]), (2, dpad.at[0]),
                   (3, khalo.at[1]), (4, vhalo.at[1]), (5, dpad.at[9])):
        got(ref, n)
    dup(khalo[0], k2, 0)
    dup(khalo[1], k2, 9 * BLK)
    dup(vhalo[0], v3, 0)
    dup(vhalo[1], v3, 9 * BLK)
    dpad[0] = jnp.where(s == 0, -1, dpad[0])
    dpad[9] = jnp.where(s == 63, -1, dpad[9])

    scale = HD ** (-0.5)
    m_even = jnp.where(low, scale, 0.0).astype(BF)
    m_odd = jnp.where(low, 0.0, scale).astype(BF)

    def pair_of_blocks(t, out, out_at):
        p = lax.rem(y + 1 + t, 4)

        @pl.loop(0, 2)
        def _(sub):
            b = 2 * p + sub
            at = pl.multiple_of(b * BLK, BLK)
            qd = jnp.transpose(jnp.broadcast_to(dpad[b + 1].astype(F32), (BLK, BLK)))
            for j in range(3):
                ok = qd == dpad[b + j].astype(F32)
                if j == 0:
                    ok = ok & (lane >= row)
                if j == 2:
                    ok = ok & (lane <= row)
                bias[:, j * BLK:(j + 1) * BLK] = jnp.where(ok, 0.0, NEG)
            for g in range(2):
                keys = k2[g, pl.ds(at, 3 * BLK), :]
                qs = []
                for pair in range(2):
                    lo_col = g * 256 + pair * BLK
                    qq = q_ref[pl.ds(at, BLK), lo_col:lo_col + BLK]
                    qs += [qq * m_even, qq * m_odd]
                sc = lax.dot_general(jnp.concatenate(qs, axis=0), keys, (((1,), (1,)), ((), ())),
                                     preferred_element_type=F32)
                for h in range(4):
                    scores[g, h * BLK:(h + 1) * BLK, :] = sc[h * BLK:(h + 1) * BLK, :] + bias[...]
            extra = {}
            for g in range(2):
                for h in range(4):
                    sink = sink_ref[g * 4 + h]
                    sc = scores[g, h * BLK:(h + 1) * BLK, :]
                    top = jnp.maximum(jnp.max(sc, axis=1, keepdims=True), sink)
                    probs[g, h * BLK:(h + 1) * BLK, :] = jnp.exp(sc - top).astype(BF)
                    extra[g, h] = jnp.exp(sink - top)
            for g in range(2):
                o = jnp.dot(probs[g], v3[g, pl.ds(at, 3 * BLK), :], preferred_element_type=F32)
                for pair in range(2):
                    res = []
                    for half in range(2):
                        h = 2 * pair + half
                        oh = o[h * BLK:(h + 1) * BLK, :]
                        res.append(oh[:, 0:BLK] / (oh[:, BLK:2 * BLK] + extra[g, h]))
                    lo_col = g * 256 + pair * BLK
                    out[out_at, pl.ds(pl.multiple_of(sub * BLK, BLK), BLK), lo_col:lo_col + BLK] = (
                        jnp.where(low, res[0], res[1]).astype(BF))

    def send_att(t):
        r = t + 1
        go(att.at[t], regr.at[4 - r], 26 + t, tps[r])

    ab, dd = pl.ds(0, 2), pl.ds(2, 1)
    parts = (ab, dd)

    def zsend(step, sh):
        for d in range(2):
            zz = z - (step - 1) if d == 0 else z + (step - 1)
            rr = rows_b(zz, c)
            ref = wall.at[parts[sh], rr] if step < 4 else wall.at[parts[sh], rr, (left, right)[d]]
            go(ref, ref, 34 + (d * 2 + sh) * 4 + step - 1, (z_next, z_prev)[d])

    def zgot(step, sh):
        for d in range(2):
            zz = z - step if d == 0 else z + step
            rr = rows_b(zz, c)
            ref = wall.at[parts[sh], rr] if step < 4 else wall.at[parts[sh], rr, (left, right)[d]]
            got(ref, 34 + (d * 2 + sh) * 4 + step - 1)

    allw = pl.ds(0, 3)
    zorder = (0, -1, 1, -2, 2, -3, 3, 4)

    def zsib(dz):
        rr = rows_b(z + dz, c)
        go(wall.at[allw, rr], wall.at[allw, rr], 50 + zorder.index(dz), sib)

    def xsib(n, xx):
        rr = rows_a(xx, c, 0, 32)
        go(wall.at[allw, rr], wall.at[allw, rr], 18 + n, sib)

    from_m, from_p = rows_a(xm, c, 0, 32), rows_a(xp, c, 0, 32)
    fm_lo, fp_hi = rows_a(xm, c, 0, 16), rows_a(xp, c, 16, 16)
    far, far_lo, far_hi = rows_a(xo, c, 0, 32), rows_a(xo, c, 0, 16), rows_a(xo, c, 16, 16)

    def xsend(sh):
        ref = wall.at[parts[sh], mine]
        go(ref, ref, 10 + 2 * sh, x_next)
        go(ref, ref, 11 + 2 * sh, x_prev)

    def xforward(sh):
        got(wall.at[parts[sh], from_m], 10 + 2 * sh)
        got(wall.at[parts[sh], from_p], 11 + 2 * sh)
        ref = wall.at[parts[sh], fm_lo]
        go(ref, ref, 14 + 2 * sh, x_next)
        ref = wall.at[parts[sh], fp_hi]
        go(ref, ref, 15 + 2 * sh, x_prev)

    pair_of_blocks(0, att, 0)
    got(wall.at[0, mine], 6)
    go(wall.at[0, mine_lo], wall.at[2, mine_lo], 8, tps[1])
    got(wall.at[1, mine], 7)
    go(wall.at[1, mine_hi], wall.at[2, mine_hi], 9, tps[3])
    got(wall.at[0, mine_b], 30)
    go(wall.at[0, mine_b, left], wall.at[2, mine_b, left], 32, tps[1])
    got(wall.at[1, mine_b], 31)
    go(wall.at[1, mine_b, right], wall.at[2, mine_b, right], 33, tps[3])
    xsend(0)
    zsend(1, 0)
    pair_of_blocks(1, att, 1)
    send_att(0)
    got(wall.at[2, mine_lo], 8)
    got(wall.at[2, mine_hi], 9)
    got(wall.at[2, mine_b, left], 32)
    got(wall.at[2, mine_b, right], 33)
    xsend(1)
    zsend(1, 1)
    xsib(0, x)
    zsib(0)
    zgot(1, 0)
    zsend(2, 0)
    pair_of_blocks(2, att, 2)
    send_att(1)
    xforward(0)
    zgot(1, 1)
    zsend(2, 1)
    zgot(2, 0)
    zsend(3, 0)
    pair_of_blocks(3, regr, 0)
    send_att(2)
    xforward(1)
    zgot(2, 1)
    zsend(3, 1)
    zgot(3, 0)
    zsend(4, 0)
    xsib(1, xm)
    xsib(2, xp)
    for dz in (-1, 1, -2, 2):
        zsib(dz)

    r_copy.wait()

    def project(r, wref, first=False):
        @pl.loop(0, 4)
        def _(n):
            cols = pl.ds(pl.multiple_of(n * 512, 512), 512)
            part = jnp.dot(regr[r], wref[:, cols], preferred_element_type=F32)
            base = resid[:, cols].astype(F32) if first else acc[:, cols]
            acc[:, cols] = base + part.astype(BF).astype(F32)

    project(0, w_own, True)
    zgot(3, 1)
    zsend(4, 1)
    zsib(-3)
    zsib(3)
    for sh in range(2):
        got(wall.at[parts[sh], far_lo], 14 + 2 * sh)
        got(wall.at[parts[sh], far_hi], 15 + 2 * sh)
    xsib(3, xo)
    zgot(4, 0)
    zgot(4, 1)
    zsib(4)
    for n, xx in enumerate((x, xm, xp, xo)):
        got(wall.at[allw, rows_a(xx, 1 - c, 0, 32)], 18 + n)
    for n, dz in enumerate(zorder):
        got(wall.at[allw, rows_b(z + dz, 1 - c)], 50 + n)
    got(regr.at[1], 28)
    got(regr.at[3], 26)
    got(regr.at[2], 27)
    project(1, wall.at[1])
    project(3, wall.at[0])
    squares[...] = jnp.zeros((256, BLK), F32)

    @pl.loop(0, 4)
    def _(n):
        cols = pl.ds(pl.multiple_of(n * 512, 512), 512)
        part = jnp.dot(regr[2], wall[2, :, cols], preferred_element_type=F32)
        st = (acc[:, cols] + part.astype(BF).astype(F32)).astype(BF)
        stream[:, cols] = st
        sq = st.astype(F32) * st.astype(F32)
        squares[...] += (sq[:, 0:128] + sq[:, 128:256]) + (sq[:, 256:384] + sq[:, 384:512])

    rms = lax.rsqrt(jnp.sum(squares[...], axis=1, keepdims=True) * (1.0 / 2048) + EPS)

    @pl.loop(0, 8)
    def _(n):
        cols = pl.ds(pl.multiple_of(n * 256, 256), 256)
        normed = (stream[:, cols].astype(F32) * rms * gain_ref[:, cols]).astype(BF)
        out = jnp.dot(pg_n[...], normed, preferred_element_type=F32).astype(BF)
        for g in range(4):
            sbuf[g, :, cols] = out[64 * g:64 * (g + 1), :]

    g_of = [g_me, lax.rem(g_me + sgn + 4, 4), lax.rem(g_me - sgn + 4, 4), lax.rem(g_me + 2, 4)]
    t_of = [None, z + sgn, z - 2 * sgn, z + 3 * sgn]
    mgo(sbuf.at[g_of[1]], land.at[1], 9, zdev(t_of[1]))
    mgo(sbuf.at[g_of[2]], land.at[2], 10, zdev(t_of[2]))
    mgo(sbuf.at[g_of[3]], land.at[3], 11, zdev(t_of[3]))
    for o in range(1, 8):
        mgot(metar.at[o], o)

    def origin(b):
        if b == 0:
            return 0
        if b < 4:
            return lax.rem(8 - sgn * b, 8)
        return lax.rem(8 + sgn * (b - 3), 8)

    def fwd(k):
        mgot(land.at[k], 8 + k)
        mgo(land.at[k], land.at[4 + k], 11 + k, partner)

    ii = lax.broadcasted_iota(jnp.int32, (128, 128), 0)

    def exchange(p):
        b0, b1 = PAIRS[p]
        mm = jnp.where(lane[0:8, :] < 64, metar[origin(b0)], metar[origin(b1)])
        slot = ((((ii >> 4) + me) & 7) << 3) + (ii & 7) + 64 * zl
        slot = jnp.where(((ii >> 3) & 1) == (lane >> 6), slot, -1).astype(F32)
        hit0 = slot == mm[0:1, :]
        hit1 = slot == mm[1:2, :]
        sel = jnp.where(hit0 | hit1, 1.0, 0.0).astype(BF)
        for r, ref in ((2, whi), (3, wlo)):
            wt = jnp.where(hit0, mm[r:r + 1, :], 0.0) + jnp.where(hit1, mm[r + 2:r + 3, :], 0.0)
            ref[p] = jnp.transpose(wt).astype(BF)
        first = sbuf.at[g_me] if b0 == 0 else land.at[b0]

        @pl.loop(0, 4)
        def _(n):
            cols = pl.ds(pl.multiple_of(n * 512, 512), 512)
            rows = jnp.concatenate([first[:, cols], land[b1, :, cols]], axis=0)
            out = jnp.dot(sel, rows, preferred_element_type=F32).astype(BF)
            xbuf[p, :, cols] = out
            xin[p, 0:16, cols] = out[0:16, :]

        for o in (2, 6, 4, 5, 3, 7, 1):
            sl = pl.ds(16 * o, 16)
            mgo(xbuf.at[p, sl], xin.at[p, sl], 15 + p, xdev(me + o), note=False)

    rest = pl.ds(16, 112)

    def expert(p):
        mgot(xin.at[p, rest], 15 + p)
        rows = xin[p]
        gate_act = jnp.dot(rows, wg[...], preferred_element_type=F32)
        up_act = jnp.dot(rows, wu[...], preferred_element_type=F32)
        hidden = (gate_act / (1.0 + jnp.exp(-gate_act)) * up_act).astype(BF)

        @pl.loop(0, 4)
        def _(n):
            cols = pl.ds(pl.multiple_of(n * 512, 512), 512)
            out = jnp.dot(hidden, wd[:, cols], preferred_element_type=F32).astype(BF)
            pbuf[p, :, cols] = out
            rbuf[p, 0:16, cols] = out[0:16, :]

        for o in (2, 6, 4, 5, 3, 7, 1):
            sl = pl.ds(16 * o, 16)
            mgo(pbuf.at[p, sl], rbuf.at[p, sl], 19 + p, xdev(me - o), note=False)

    def merge(p):
        mgot(rbuf.at[p, rest], 19 + p)

        @pl.loop(0, 4)
        def _(n):
            cols = pl.ds(pl.multiple_of(n * 512, 512), 512)
            rows = rbuf[p, :, cols]
            out = (jnp.dot(whi[p], rows, preferred_element_type=F32)
                   + jnp.dot(wlo[p], rows, preferred_element_type=F32))
            for h, b in enumerate(PAIRS[p]):
                piece = out[64 * h:64 * (h + 1), :]
                if b < 4:
                    partk[b, :, cols] = piece
                else:
                    psend[b - 4, :, cols] = piece.astype(BF)

        for b in PAIRS[p]:
            if b >= 4:
                mgo(psend.at[b - 4], cback.at[b - 4], 19 + b, partner)

    def total(j):
        mgot(cback.at[j], 23 + j)

        @pl.loop(0, 4)
        def _(n):
            cols = pl.ds(pl.multiple_of(n * 512, 512), 512)
            out = (partk[j, :, cols] + cback[j, :, cols].astype(F32)).astype(BF)
            if j == 0:
                fin[g_me, :, cols] = out
            else:
                totb[j - 1, :, cols] = out

        if j:
            mgo(totb.at[j - 1], fin.at[g_me], 26 + j, zdev(z + sgn * j))

    for cp in loads:
        cp.wait()
    fwd(1)
    exchange(0)
    fwd(2)
    fwd(3)
    mgo(sbuf.at[g_me], land.at[4], 8, partner)
    exchange(1)
    expert(0)
    mgot(land.at[5], 12)
    mgot(land.at[6], 13)
    exchange(2)
    expert(1)
    merge(0)
    expert(2)
    merge(1)
    mgot(land.at[7], 14)
    mgot(land.at[4], 8)
    exchange(3)
    merge(2)
    expert(3)
    total(1)
    total(2)
    merge(3)
    total(3)
    total(0)
    for k in (1, 2, 3):
        mgot(fin.at[g_of[k]], 26 + k)

    @pl.loop(0, 8)
    def _(n):
        cols = pl.ds(pl.multiple_of(n * 256, 256), 256)
        out = stream[:, cols].astype(F32)
        rows = jnp.concatenate([fin[g, :, cols] for g in range(4)], axis=0)
        out += jnp.dot(pg_t[...], rows, preferred_element_type=F32)
        mixed_ref[:, cols] = out.astype(BF)

    for d in pending:
        d.wait_send()
    for p in range(4):
        mrc(xbuf.at[p, rest], xbuf.at[p, rest], 15 + p, partner).wait_send()
        mrc(pbuf.at[p, rest], pbuf.at[p, rest], 19 + p, partner).wait_send()


def layer(queries, key_rows, value_rows, doc_ids, sink_logit, residual, out_weight, norm_gain,
          gate_weight, up_weight, down_weight, routes, route_weights):
    vm = pl.BlockSpec(memory_space=pltpu.VMEM)
    anyspec = pl.BlockSpec(memory_space=pl.ANY)
    smem = pl.BlockSpec(memory_space=pltpu.SMEM)
    big = (4, 128, 2048)
    rows4 = (4, 64, 2048)
    dma = pltpu.SemaphoreType.DMA
    return pl.pallas_call(
        layer_kernel,
        out_shape=jax.ShapeDtypeStruct((256, 2048), BF),
        in_specs=[vm, vm, vm, vm, smem, vm, vm, vm] + [anyspec] * 5,
        out_specs=vm,
        scratch_shapes=[
            pltpu.VMEM((2, 1280, 128), BF),
            pltpu.VMEM((2, 1280, 256), BF),
            pltpu.VMEM((10, 1, 128), jnp.int32),
            pltpu.VMEM((2, 128, 128), BF),
            pltpu.VMEM((2, 128, 128), BF),
            pltpu.VMEM((3, 256, 512), BF),
            pltpu.VMEM((4, 256, 512), BF),
            pltpu.VMEM((3, 512, 2048), BF),
            pltpu.VMEM((512, 2048), BF),
            pltpu.VMEM((256, 2048), BF),
            pltpu.VMEM((256, 2048), F32),
            pltpu.VMEM((128, 384), F32),
            pltpu.VMEM((2, 512, 384), F32),
            pltpu.VMEM((2, 512, 384), BF),
            pltpu.VMEM((256, 128), F32),
            pltpu.VMEM((256, 2048), BF),
            pltpu.VMEM(rows4, BF),
            pltpu.VMEM((8, 64, 2048), BF),
            pltpu.VMEM((4, 8, 128), F32),
            pltpu.VMEM((8, 8, 128), F32),
            pltpu.VMEM((16, 256), F32),
            pltpu.VMEM((256, 256), BF),
            pltpu.VMEM((256, 256), BF),
            pltpu.VMEM((4, 128, 128), BF),
            pltpu.VMEM((4, 128, 128), BF),
            pltpu.VMEM(big, BF),
            pltpu.VMEM(big, BF),
            pltpu.VMEM(big, BF),
            pltpu.VMEM(big, BF),
            pltpu.VMEM(rows4, F32),
            pltpu.VMEM(rows4, BF),
            pltpu.VMEM(rows4, BF),
            pltpu.VMEM((3, 64, 2048), BF),
            pltpu.VMEM(rows4, BF),
            pltpu.VMEM((2048, 512), BF),
            pltpu.VMEM((2048, 512), BF),
            pltpu.VMEM((512, 2048), BF),
            dma((58,)), dma((58,)), dma((30,)), dma((30,)), dma((5,)),
        ],
        compiler_params=pltpu.CompilerParams(
            collective_id=0, has_side_effects=True, vmem_limit_bytes=62 * 2**20
        ),
        name="layer",
    )(
        queries, key_rows, value_rows, doc_ids.reshape(8, 1, 128), sink_logit,
        norm_gain.reshape(1, 2048), routes.T, route_weights.T, residual, out_weight,
        gate_weight, up_weight, down_weight,
    )


def per_device(
    queries,
    key_rows,
    value_rows,
    doc_ids,
    sink_logit,
    residual,
    out_weight,
    norm_gain,
    gate_weight,
    up_weight,
    down_weight,
    routes,
    route_weights,
):
    return layer(
        queries, key_rows, value_rows, doc_ids, sink_logit, residual, out_weight, norm_gain,
        gate_weight, up_weight, down_weight, routes, route_weights,
    )


def solution(mesh):
    return jax.shard_map(
        per_device,
        mesh=mesh,
        in_specs=(
            P("sp", "tp"),
            P("sp", "tp"),
            P("sp", "tp"),
            P("sp"),
            P("tp"),
            P(("sp", "tp"), None),
            P("tp", None),
            P(),
            P("sp", None, None),
            P("sp", None, None),
            P("sp", None, None),
            P(("sp", "tp"), None),
            P(("sp", "tp"), None),
        ),
        out_specs=P(("sp", "tp"), None),
        check_vma=False,
    )
```

time: 214 us -> 151 us (0.71)
  Pallas kernels: 51.2 us -> 146 us
  blocking collectives: 60.5 us -> 0 us
  waiting for transfers between devices: 51 us -> 0 us
  local copies, waits for them, and re-layouts: 24.8 us -> 2.3 us
  other arithmetic: 12.5 us -> 0 us
  matrix products: 7.24 us -> 0 us
  starting transfers between devices: 5.94 us -> 0 us
    pallas_call x1, Pallas kernels: 51.2 us -> 146 us  [layer(): pl.pallas_call(layer_kernel, out_shape=jax.ShapeDtypeStruct((256, 2048),...]
    all_to_all x1 -> x0, blocking collectives: 60.5 us -> none  [per_device(): lax.all_to_all(outgoing, 'sp', split_axis=0, concat_axis=0, tiled=True)]
    all_to_all x1 -> x0, waiting for transfers between devices: 51 us -> none  [per_device(): lax.all_to_all(produced.reshape(incoming.shape), 'sp', split_axis=0, conc...]
    gather x2 -> x0, local copies, waits for them, and re-layouts: 13.8 us -> none  [the longest x1 7.13 us: per_device(): returned.reshape(-1, width)[slot_index]]
    reduce_sum x2 -> x0, other arithmetic: 9.09 us -> none  [the longest x1 8.96 us: per_device(): jnp.sum(route_weights[:, :, None] * route_out.astype(jnp.float32), axis=1)]
    dot_general x2 -> x0, matrix products: 7.24 us -> none  [the longest x1 6 us: per_device(): jnp.dot(hidden, down_weight[0], preferred_element_type=jnp.float32)]
    all_to_all x1 -> x0, starting transfers between devices: 5.94 us -> none  [per_device(): lax.all_to_all(produced.reshape(incoming.shape), 'sp', split_axis=0, conc...]
    convert_element_type x1 -> x0, local copies, waits for them, and re-layouts: 5.44 us -> none  [per_device(): route_out.astype(jnp.float32)]
  transfers between devices with their start and end apart: 1 -> 0, of which waited for: 1 -> 0; matrix products, arithmetic and copies ran while one was open for 0% -> 0% of each run, Pallas kernels for 0% -> 0%
where the time goes in v3:
time: 151 us; the launch traced here: 148 us
  Pallas kernels  146 us (97%)
  local copies, waits for them, and re-layouts  2.3 us (2%)
    pallas_call x1, Pallas kernels, layer(): pl.pallas_call(layer_kernel, out_shape=jax.ShapeDtypeStruct((256, 2048),...  146 us

profile of v3, /device:TPU:2, one launch (start us, length us, event | category | flops | bytes accessed | tf_op | source)
XLA Modules:
  0.0 148.1 jit_solution(8925543424947663313)
XLA Ops:
  0.0 145.8 %layer.1 = bf16[256,2048]{1,0:T(8,128)(2,1)} custom-call(bf16[1024,512]{1,0:T(8,128)(2,1)} %q_ref.1, bf16[1024,128]{1,0:T(8,128)(2,1)} %k_ref.1, bf16[1024,128]{1,0:T(8,128)(2,1)} %v_ref.1, s32[8,1,128]{2,1,0:T(1,128)} %bitcast.5, f32[8]{0:T(128)} %sink_ref.1, f32[1,2048]{1,0:T(1,128)} %bitcast.4, s32[2,256]{1,0:T(2,128)} %bitcast.6, f32[2,256]{1,0:T(2,128)} %bitcast.7, ...), custom_call_target="tpu_custom_call" | custom-call | tf_op jit(solution)/shard_map/layer/pallas_call | solution.py:554
  145.8 2.3 %copy.15 = bf16[256,2048]{1,0:T(8,128)(2,1)} copy(bf16[256,2048]{1,0:T(8,128)(2,1)} %layer.1) | data formatting | bytes 2097152

commit v4 on v3

--- a/solution.py
+++ b/solution.py
@@ -27,7 +27,7 @@
     return (z * 4 + x) * 2 + c
 
 
-PAIRS = ((0, 1), (2, 3), (5, 6), (7, 4))
+PAIRS = ((0, 1), (2, 4), (6, 7), (3, 5))
 
 
 def layer_kernel(
@@ -36,7 +36,7 @@
     mixed_ref,
     k2, v3, dpad, khalo, vhalo, att, regr, wall, w_own, resid, acc, bias, scores, probs, squares,
     stream, sbuf, land, metas, metar, mscr, pg_n, pg_t, whi, wlo, xbuf, xin, pbuf, rbuf,
-    partk, psend, cback, totb, fin, wg, wu, wd, fsend, frecv, msend, mrecv, lsem,
+    partk, psend, cback, totb, fin, fin2, wg, wu, wd, fsend, frecv, msend, mrecv, lsem,
 ):
     s, y, z, x, c = coords()
     xm, xp = lax.rem(x + 3, 4), lax.rem(x + 1, 4)
@@ -107,31 +107,6 @@
     greet += [zdev(z + o) for o in range(1, 8)] + [xdev(me + o) for o in range(1, 8)]
     for dev in greet:
         pl.semaphore_signal(barrier, inc=1, device_id=dev, device_id_type=MESH)
-    pl.semaphore_wait(barrier, len(greet))
-
-    go(k_ref.at[pl.ds(896, 128)], khalo.at[0], 0, sp_next)
-    go(v_ref.at[pl.ds(896, 128)], vhalo.at[0], 1, sp_next)
-    go(docs_ref.at[7], dpad.at[0], 2, sp_next)
-    go(k_ref.at[pl.ds(0, 128)], khalo.at[1], 3, sp_prev)
-    go(v_ref.at[pl.ds(0, 128)], vhalo.at[1], 4, sp_prev)
-    go(docs_ref.at[0], dpad.at[9], 5, sp_prev)
-
-    def rows_a(xx, cc, off, n):
-        return pl.ds(pl.multiple_of(64 * xx + 32 * cc + off, 16), n)
-
-    def rows_b(zz, cc):
-        return pl.ds(pl.multiple_of(256 + 32 * lax.rem(zz + 16, 8) + 16 * cc, 16), 16)
-
-    left, right = pl.ds(0, 1024), pl.ds(1024, 1024)
-    w_copy.wait()
-    mine = rows_a(x, c, 0, 32)
-    mine_lo, mine_hi = rows_a(x, c, 0, 16), rows_a(x, c, 16, 16)
-    mine_b = rows_b(z, c)
-    go(w_own.at[mine], wall.at[0, mine], 6, tps[1])
-    go(w_own.at[mine], wall.at[1, mine], 7, tps[3])
-    go(w_own.at[mine_b], wall.at[0, mine_b], 30, tps[1])
-    go(w_own.at[mine_b], wall.at[1, mine_b], 31, tps[3])
-
     e0, e1 = routes_ref[0:1, :], routes_ref[1:2, :]
     upper = (lax.broadcasted_iota(jnp.int32, (256, 256), 0)
              < lax.broadcasted_iota(jnp.int32, (256, 256), 1)).astype(F32).astype(BF)
@@ -167,11 +142,6 @@
         metas[g] = lax.dot_general(info, both, (((1,), (1,)), ((), ())),
                                    preferred_element_type=F32)[0:8, :]
 
-    for o in range(1, 8):
-        zz = lax.rem(z + o, 8)
-        mgo(metas.at[zz // 2], metar.at[o], o, zdev(z + o))
-    metar[0] = metas[g_me]
-
     lane = lax.broadcasted_iota(jnp.int32, (BLK, BLK), 1)
     row = lax.broadcasted_iota(jnp.int32, (BLK, BLK), 0)
     low = lane < 64
@@ -194,6 +164,36 @@
         at = pl.multiple_of(i * BLK, BLK)
         for g in range(2):
             v3[g, pl.ds(at, BLK), BLK:2 * BLK] = jnp.ones((BLK, BLK), BF)
+
+    pl.semaphore_wait(barrier, len(greet))
+
+    go(k_ref.at[pl.ds(896, 128)], khalo.at[0], 0, sp_next)
+    go(v_ref.at[pl.ds(896, 128)], vhalo.at[0], 1, sp_next)
+    go(docs_ref.at[7], dpad.at[0], 2, sp_next)
+    go(k_ref.at[pl.ds(0, 128)], khalo.at[1], 3, sp_prev)
+    go(v_ref.at[pl.ds(0, 128)], vhalo.at[1], 4, sp_prev)
+    go(docs_ref.at[0], dpad.at[9], 5, sp_prev)
+
+    def rows_a(xx, cc, off, n):
+        return pl.ds(pl.multiple_of(64 * xx + 32 * cc + off, 16), n)
+
+    def rows_b(zz, cc):
+        return pl.ds(pl.multiple_of(256 + 32 * lax.rem(zz + 16, 8) + 16 * cc, 16), 16)
+
+    left, right = pl.ds(0, 1024), pl.ds(1024, 1024)
+    w_copy.wait()
+    mine = rows_a(x, c, 0, 32)
+    mine_lo, mine_hi = rows_a(x, c, 0, 16), rows_a(x, c, 16, 16)
+    mine_b = rows_b(z, c)
+    go(w_own.at[mine], wall.at[0, mine], 6, tps[1])
+    go(w_own.at[mine], wall.at[1, mine], 7, tps[3])
+    go(w_own.at[mine_b], wall.at[0, mine_b], 30, tps[1])
+    go(w_own.at[mine_b], wall.at[1, mine_b], 31, tps[3])
+
+    for o in range(1, 8):
+        zz = lax.rem(z + o, 8)
+        mgo(metas.at[zz // 2], metar.at[o], o, zdev(z + o))
+    metar[0] = metas[g_me]
 
     for n, ref in ((0, khalo.at[0]), (1, vhalo.at[0]), (2, dpad.at[0]),
                    (3, khalo.at[1]), (4, vhalo.at[1]), (5, dpad.at[9])):
@@ -276,16 +276,23 @@
             ref = wall.at[parts[sh], rr] if step < 4 else wall.at[parts[sh], rr, (left, right)[d]]
             got(ref, 34 + (d * 2 + sh) * 4 + step - 1)
 
-    allw = pl.ds(0, 3)
     zorder = (0, -1, 1, -2, 2, -3, 3, 4)
 
-    def zsib(dz):
-        rr = rows_b(z + dz, c)
-        go(wall.at[allw, rr], wall.at[allw, rr], 50 + zorder.index(dz), sib)
-
-    def xsib(n, xx):
-        rr = rows_a(xx, c, 0, 32)
-        go(wall.at[allw, rr], wall.at[allw, rr], 18 + n, sib)
+    def zsib(sh, *dzs):
+        for dz in dzs:
+            ref = wall.at[parts[sh], rows_b(z + dz, c)]
+            go(ref, ref, 68 + 2 * zorder.index(dz) + sh, sib)
+
+    def xsib(sh, *ns):
+        for n in ns:
+            ref = wall.at[parts[sh], rows_a((x, xm, xp, xo)[n], c, 0, 32)]
+            go(ref, ref, 60 + 2 * n + sh, sib)
+
+    def sib_done(sh):
+        for n, xx in enumerate((x, xm, xp, xo)):
+            got(wall.at[parts[sh], rows_a(xx, 1 - c, 0, 32)], 60 + 2 * n + sh)
+        for n, dz in enumerate(zorder):
+            got(wall.at[parts[sh], rows_b(z + dz, 1 - c)], 68 + 2 * n + sh)
 
     from_m, from_p = rows_a(xm, c, 0, 32), rows_a(xp, c, 0, 32)
     fm_lo, fp_hi = rows_a(xm, c, 0, 16), rows_a(xp, c, 16, 16)
@@ -323,8 +330,9 @@
     got(wall.at[2, mine_b, right], 33)
     xsend(1)
     zsend(1, 1)
-    xsib(0, x)
-    zsib(0)
+    for sh in range(2):
+        xsib(sh, 0)
+        zsib(sh, 0)
     zgot(1, 0)
     zsend(2, 0)
     pair_of_blocks(2, att, 2)
@@ -341,15 +349,15 @@
     zsend(3, 1)
     zgot(3, 0)
     zsend(4, 0)
-    xsib(1, xm)
-    xsib(2, xp)
-    for dz in (-1, 1, -2, 2):
-        zsib(dz)
+    for sh in range(2):
+        xsib(sh, 1, 2)
+        zsib(sh, -1, 1, -2, 2)
+    zsib(0, -3, 3)
 
     r_copy.wait()
 
     def project(r, wref, first=False):
-        @pl.loop(0, 4)
+        @pl.loop(0, 4, unroll=True)
         def _(n):
             cols = pl.ds(pl.multiple_of(n * 512, 512), 512)
             part = jnp.dot(regr[r], wref[:, cols], preferred_element_type=F32)
@@ -359,27 +367,27 @@
     project(0, w_own, True)
     zgot(3, 1)
     zsend(4, 1)
-    zsib(-3)
-    zsib(3)
-    for sh in range(2):
+    zsib(1, -3, 3)
+
+    def last(sh):
         got(wall.at[parts[sh], far_lo], 14 + 2 * sh)
         got(wall.at[parts[sh], far_hi], 15 + 2 * sh)
-    xsib(3, xo)
-    zgot(4, 0)
-    zgot(4, 1)
-    zsib(4)
-    for n, xx in enumerate((x, xm, xp, xo)):
-        got(wall.at[allw, rows_a(xx, 1 - c, 0, 32)], 18 + n)
-    for n, dz in enumerate(zorder):
-        got(wall.at[allw, rows_b(z + dz, 1 - c)], 50 + n)
+        xsib(sh, 3)
+        zgot(4, sh)
+        zsib(sh, 4)
+
+    last(0)
+    last(1)
+    sib_done(0)
     got(regr.at[1], 28)
     got(regr.at[3], 26)
-    got(regr.at[2], 27)
     project(1, wall.at[1])
     project(3, wall.at[0])
+    got(regr.at[2], 27)
+    sib_done(1)
     squares[...] = jnp.zeros((256, BLK), F32)
 
-    @pl.loop(0, 4)
+    @pl.loop(0, 4, unroll=True)
     def _(n):
         cols = pl.ds(pl.multiple_of(n * 512, 512), 512)
         part = jnp.dot(regr[2], wall[2, :, cols], preferred_element_type=F32)
@@ -390,7 +398,7 @@
 
     rms = lax.rsqrt(jnp.sum(squares[...], axis=1, keepdims=True) * (1.0 / 2048) + EPS)
 
-    @pl.loop(0, 8)
+    @pl.loop(0, 8, unroll=4)
     def _(n):
         cols = pl.ds(pl.multiple_of(n * 256, 256), 256)
         normed = (stream[:, cols].astype(F32) * rms * gain_ref[:, cols]).astype(BF)
@@ -403,6 +411,7 @@
     mgo(sbuf.at[g_of[1]], land.at[1], 9, zdev(t_of[1]))
     mgo(sbuf.at[g_of[2]], land.at[2], 10, zdev(t_of[2]))
     mgo(sbuf.at[g_of[3]], land.at[3], 11, zdev(t_of[3]))
+    mgo(sbuf.at[g_me], land.at[4], 8, partner)
     for o in range(1, 8):
         mgot(metar.at[o], o)
 
@@ -414,7 +423,6 @@
         return lax.rem(8 + sgn * (b - 3), 8)
 
     def fwd(k):
-        mgot(land.at[k], 8 + k)
         mgo(land.at[k], land.at[4 + k], 11 + k, partner)
 
     ii = lax.broadcasted_iota(jnp.int32, (128, 128), 0)
@@ -445,6 +453,7 @@
             mgo(xbuf.at[p, sl], xin.at[p, sl], 15 + p, xdev(me + o), note=False)
 
     rest = pl.ds(16, 112)
+    half = (pl.ds(0, 1024), pl.ds(1024, 1024))
 
     def expert(p):
         mgot(xin.at[p, rest], 15 + p)
@@ -453,21 +462,23 @@
         up_act = jnp.dot(rows, wu[...], preferred_element_type=F32)
         hidden = (gate_act / (1.0 + jnp.exp(-gate_act)) * up_act).astype(BF)
 
-        @pl.loop(0, 4)
-        def _(n):
-            cols = pl.ds(pl.multiple_of(n * 512, 512), 512)
-            out = jnp.dot(hidden, wd[:, cols], preferred_element_type=F32).astype(BF)
-            pbuf[p, :, cols] = out
-            rbuf[p, 0:16, cols] = out[0:16, :]
-
-        for o in (2, 6, 4, 5, 3, 7, 1):
-            sl = pl.ds(16 * o, 16)
-            mgo(pbuf.at[p, sl], rbuf.at[p, sl], 19 + p, xdev(me - o), note=False)
-
-    def merge(p):
-        mgot(rbuf.at[p, rest], 19 + p)
-
-        @pl.loop(0, 4)
+        for ch in range(2):
+            @pl.loop(2 * ch, 2 * ch + 2, unroll=True)
+            def _(n):
+                cols = pl.ds(pl.multiple_of(n * 512, 512), 512)
+                out = jnp.dot(hidden, wd[:, cols], preferred_element_type=F32).astype(BF)
+                pbuf[p, :, cols] = out
+                rbuf[p, 0:16, cols] = out[0:16, :]
+
+            for o in (2, 6, 4, 5, 3, 7, 1):
+                sl = pl.ds(16 * o, 16)
+                mgo(pbuf.at[p, sl, half[ch]], rbuf.at[p, sl, half[ch]], 30 + 2 * p + ch, xdev(me - o), note=False)
+
+    def merge(p, ch):
+        hc = half[ch]
+        mgot(rbuf.at[p, rest, hc], 30 + 2 * p + ch)
+
+        @pl.loop(2 * ch, 2 * ch + 2, unroll=True)
         def _(n):
             cols = pl.ds(pl.multiple_of(n * 512, 512), 512)
             rows = rbuf[p, :, cols]
@@ -475,72 +486,88 @@
                    + jnp.dot(wlo[p], rows, preferred_element_type=F32))
             for h, b in enumerate(PAIRS[p]):
                 piece = out[64 * h:64 * (h + 1), :]
-                if b < 4:
+                if b == 0:
+                    fin[g_me, :, cols] = piece.astype(BF)
+                elif b == 1:
+                    totb[0, :, cols] = piece.astype(BF)
+                elif b < 4:
                     partk[b, :, cols] = piece
                 else:
                     psend[b - 4, :, cols] = piece.astype(BF)
 
-        for b in PAIRS[p]:
-            if b >= 4:
-                mgo(psend.at[b - 4], cback.at[b - 4], 19 + b, partner)
-
-    def total(j):
-        mgot(cback.at[j], 23 + j)
-
-        @pl.loop(0, 4)
-        def _(n):
-            cols = pl.ds(pl.multiple_of(n * 512, 512), 512)
-            out = (partk[j, :, cols] + cback[j, :, cols].astype(F32)).astype(BF)
-            if j == 0:
-                fin[g_me, :, cols] = out
-            else:
-                totb[j - 1, :, cols] = out
-
-        if j:
-            mgo(totb.at[j - 1], fin.at[g_me], 26 + j, zdev(z + sgn * j))
+        for b in reversed(PAIRS[p]):
+            n = 38 + 2 * (b - 4) + ch
+            if b == 1:
+                mgo(totb.at[0, :, hc], fin.at[g_me, :, hc], 46 + ch, zdev(z + sgn))
+            elif b == 4:
+                mgo(psend.at[0, :, hc], fin2.at[g_me, :, hc], n, partner)
+            elif b == 5:
+                mgo(psend.at[1, :, hc], fin2.at[g_me, :, hc], n, zdev(z - 2 * sgn))
+            elif b > 5:
+                mgo(psend.at[b - 4, :, hc], cback.at[b - 4, :, hc], n, partner)
+
+    def total(j, ch):
+        hc = half[ch]
+        mgot(cback.at[j, :, hc], 38 + 2 * j + ch)
+        totb[j - 1, :, hc] = (partk[j, :, hc] + cback[j, :, hc].astype(F32)).astype(BF)
+        mgo(totb.at[j - 1, :, hc], fin.at[g_me, :, hc], 46 + 2 * (j - 1) + ch, zdev(z + sgn * j))
 
     for cp in loads:
         cp.wait()
-    fwd(1)
+    for k in (2, 3):
+        fin2[g_of[k]] = jnp.zeros((64, 2048), BF)
+    mgot(land.at[1], 9)
     exchange(0)
+    mgot(land.at[2], 10)
     fwd(2)
-    fwd(3)
-    mgo(sbuf.at[g_me], land.at[4], 8, partner)
+    mgot(land.at[4], 8)
     exchange(1)
     expert(0)
+    mgot(land.at[3], 11)
+    fwd(3)
+    fwd(1)
+    expert(1)
+    mgot(land.at[6], 13)
+    mgot(land.at[7], 14)
+    exchange(2)
+    merge(0, 0)
+    merge(0, 1)
+    merge(1, 0)
+    merge(1, 1)
     mgot(land.at[5], 12)
-    mgot(land.at[6], 13)
-    exchange(2)
-    expert(1)
-    merge(0)
+    exchange(3)
     expert(2)
-    merge(1)
-    mgot(land.at[7], 14)
-    mgot(land.at[4], 8)
-    exchange(3)
-    merge(2)
     expert(3)
-    total(1)
-    total(2)
-    merge(3)
-    total(3)
-    total(0)
-    for k in (1, 2, 3):
-        mgot(fin.at[g_of[k]], 26 + k)
-
-    @pl.loop(0, 8)
-    def _(n):
-        cols = pl.ds(pl.multiple_of(n * 256, 256), 256)
-        out = stream[:, cols].astype(F32)
-        rows = jnp.concatenate([fin[g, :, cols] for g in range(4)], axis=0)
-        out += jnp.dot(pg_t[...], rows, preferred_element_type=F32)
-        mixed_ref[:, cols] = out.astype(BF)
+    merge(2, 0)
+    merge(2, 1)
+    merge(3, 0)
+    total(3, 0)
+    merge(3, 1)
+    total(3, 1)
+    total(2, 0)
+    total(2, 1)
+    for ch in range(2):
+        hc = half[ch]
+        mgot(fin2.at[g_me, :, hc], 38 + ch)
+        mgot(fin2.at[g_of[1], :, hc], 40 + ch)
+        for k in (1, 2, 3):
+            mgot(fin.at[g_of[k], :, hc], 46 + 2 * (k - 1) + ch)
+
+        @pl.loop(4 * ch, 4 * ch + 4, unroll=True)
+        def _(n):
+            cols = pl.ds(pl.multiple_of(n * 256, 256), 256)
+            out = stream[:, cols].astype(F32)
+            for ref in (fin, fin2):
+                rows = jnp.concatenate([ref[g, :, cols] for g in range(4)], axis=0)
+                out += jnp.dot(pg_t[...], rows, preferred_element_type=F32)
+            mixed_ref[:, cols] = out.astype(BF)
 
     for d in pending:
         d.wait_send()
     for p in range(4):
         mrc(xbuf.at[p, rest], xbuf.at[p, rest], 15 + p, partner).wait_send()
-        mrc(pbuf.at[p, rest], pbuf.at[p, rest], 19 + p, partner).wait_send()
+        for ch in range(2):
+            mrc(pbuf.at[p, rest, half[ch]], pbuf.at[p, rest, half[ch]], 30 + 2 * p + ch, partner).wait_send()
 
 
 def layer(queries, key_rows, value_rows, doc_ids, sink_logit, residual, out_weight, norm_gain,
@@ -591,10 +618,11 @@
             pltpu.VMEM(rows4, BF),
             pltpu.VMEM((3, 64, 2048), BF),
             pltpu.VMEM(rows4, BF),
+            pltpu.VMEM(rows4, BF),
             pltpu.VMEM((2048, 512), BF),
             pltpu.VMEM((2048, 512), BF),
             pltpu.VMEM((512, 2048), BF),
-            dma((58,)), dma((58,)), dma((30,)), dma((30,)), dma((5,)),
+            dma((84,)), dma((84,)), dma((52,)), dma((52,)), dma((5,)),
         ],
         compiler_params=pltpu.CompilerParams(
             collective_id=0, has_side_effects=True, vmem_limit_bytes=62 * 2**20

time: 151 us -> 135 us (0.89)
  Pallas kernels: 146 us -> 131 us
    pallas_call x1, Pallas kernels: 146 us -> 131 us  [layer(): pl.pallas_call(layer_kernel, out_shape=jax.ShapeDtypeStruct((256, 2048),...]
where the time goes in v4:
time: 135 us; the launch traced here: 133 us
  Pallas kernels  131 us (97%)
  local copies, waits for them, and re-layouts  2.3 us (2%)
    pallas_call x1, Pallas kernels, layer(): pl.pallas_call(layer_kernel, out_shape=jax.ShapeDtypeStruct((256, 2048),...  131 us

profile of v4, /device:TPU:2, one launch (start us, length us, event | category | flops | bytes accessed | tf_op | source)
XLA Modules:
  0.0 133.4 jit_solution(12106452326777240560)
XLA Ops:
  0.0 131.1 %layer.1 = bf16[256,2048]{1,0:T(8,128)(2,1)} custom-call(bf16[1024,512]{1,0:T(8,128)(2,1)} %q_ref.1, bf16[1024,128]{1,0:T(8,128)(2,1)} %k_ref.1, bf16[1024,128]{1,0:T(8,128)(2,1)} %v_ref.1, s32[8,1,128]{2,1,0:T(1,128)} %bitcast.5, f32[8]{0:T(128)} %sink_ref.1, f32[1,2048]{1,0:T(1,128)} %bitcast.4, s32[2,256]{1,0:T(2,128)} %bitcast.6, f32[2,256]{1,0:T(2,128)} %bitcast.7, ...), custom_call_target="tpu_custom_call" | custom-call | tf_op jit(solution)/shard_map/layer/pallas_call | solution.py:581
  131.1 2.3 %copy.15 = bf16[256,2048]{1,0:T(8,128)(2,1)} copy(bf16[256,2048]{1,0:T(8,128)(2,1)} %layer.1) | data formatting | bytes 2097152

commit v5 on v4

--- a/solution.py
+++ b/solution.py
@@ -398,20 +398,32 @@
 
     rms = lax.rsqrt(jnp.sum(squares[...], axis=1, keepdims=True) * (1.0 / 2048) + EPS)
 
-    @pl.loop(0, 8, unroll=4)
-    def _(n):
-        cols = pl.ds(pl.multiple_of(n * 256, 256), 256)
-        normed = (stream[:, cols].astype(F32) * rms * gain_ref[:, cols]).astype(BF)
-        out = jnp.dot(pg_n[...], normed, preferred_element_type=F32).astype(BF)
-        for g in range(4):
-            sbuf[g, :, cols] = out[64 * g:64 * (g + 1), :]
-
+    half = (pl.ds(0, 1024), pl.ds(1024, 1024))
     g_of = [g_me, lax.rem(g_me + sgn + 4, 4), lax.rem(g_me - sgn + 4, 4), lax.rem(g_me + 2, 4)]
-    t_of = [None, z + sgn, z - 2 * sgn, z + 3 * sgn]
-    mgo(sbuf.at[g_of[1]], land.at[1], 9, zdev(t_of[1]))
-    mgo(sbuf.at[g_of[2]], land.at[2], 10, zdev(t_of[2]))
-    mgo(sbuf.at[g_of[3]], land.at[3], 11, zdev(t_of[3]))
-    mgo(sbuf.at[g_me], land.at[4], 8, partner)
+    t_of = [z - sgn, z + sgn, z - 2 * sgn, z + 3 * sgn]
+
+    def zsem(b, ch):
+        return 52 + 2 * (b - 1) + ch
+
+    def depart(k, ch):
+        hc = half[ch]
+        b = k if k else 4
+        mgo(sbuf.at[g_of[k], :, hc], land.at[b, :, hc], zsem(b, ch), zdev(t_of[k]))
+
+    for ch in range(2):
+        @pl.loop(4 * ch, 4 * ch + 4, unroll=True)
+        def _(n):
+            cols = pl.ds(pl.multiple_of(n * 256, 256), 256)
+            normed = (stream[:, cols].astype(F32) * rms * gain_ref[:, cols]).astype(BF)
+            out = jnp.dot(pg_n[...], normed, preferred_element_type=F32).astype(BF)
+            for g in range(4):
+                sbuf[g, :, cols] = out[64 * g:64 * (g + 1), :]
+
+        depart(1, ch)
+        depart(2, ch)
+    for k in (3, 0):
+        depart(k, 0)
+        depart(k, 1)
     for o in range(1, 8):
         mgot(metar.at[o], o)
 
@@ -422,12 +434,18 @@
             return lax.rem(8 - sgn * b, 8)
         return lax.rem(8 + sgn * (b - 3), 8)
 
-    def fwd(k):
-        mgo(land.at[k], land.at[4 + k], 11 + k, partner)
+    def arrive(b, ch):
+        mgot(land.at[b, :, half[ch]], zsem(b, ch))
+
+    def fwd(k, wait=True):
+        for ch in range(2):
+            if wait:
+                arrive(k, ch)
+            mgo(land.at[k, :, half[ch]], land.at[4 + k, :, half[ch]], zsem(4 + k, ch), partner)
 
     ii = lax.broadcasted_iota(jnp.int32, (128, 128), 0)
 
-    def exchange(p):
+    def exchange(p, *waits):
         b0, b1 = PAIRS[p]
         mm = jnp.where(lane[0:8, :] < 64, metar[origin(b0)], metar[origin(b1)])
         slot = ((((ii >> 4) + me) & 7) << 3) + (ii & 7) + 64 * zl
@@ -440,26 +458,33 @@
             ref[p] = jnp.transpose(wt).astype(BF)
         first = sbuf.at[g_me] if b0 == 0 else land.at[b0]
 
-        @pl.loop(0, 4)
-        def _(n):
-            cols = pl.ds(pl.multiple_of(n * 512, 512), 512)
-            rows = jnp.concatenate([first[:, cols], land[b1, :, cols]], axis=0)
-            out = jnp.dot(sel, rows, preferred_element_type=F32).astype(BF)
-            xbuf[p, :, cols] = out
-            xin[p, 0:16, cols] = out[0:16, :]
-
-        for o in (2, 6, 4, 5, 3, 7, 1):
-            sl = pl.ds(16 * o, 16)
-            mgo(xbuf.at[p, sl], xin.at[p, sl], 15 + p, xdev(me + o), note=False)
+        for ch in range(2):
+            for b in waits:
+                arrive(b, ch)
+
+            @pl.loop(2 * ch, 2 * ch + 2, unroll=True)
+            def _(n):
+                cols = pl.ds(pl.multiple_of(n * 512, 512), 512)
+                rows = jnp.concatenate([first[:, cols], land[b1, :, cols]], axis=0)
+                out = jnp.dot(sel, rows, preferred_element_type=F32).astype(BF)
+                xbuf[p, :, cols] = out
+                xin[p, 0:16, cols] = out[0:16, :]
+
+            for o in (4, 5, 3, 2, 6, 7, 1):
+                sl = pl.ds(16 * o, 16)
+                mgo(xbuf.at[p, sl, half[ch]], xin.at[p, sl, half[ch]], 66 + 2 * p + ch, xdev(me + o), note=False)
 
     rest = pl.ds(16, 112)
-    half = (pl.ds(0, 1024), pl.ds(1024, 1024))
 
     def expert(p):
-        mgot(xin.at[p, rest], 15 + p)
-        rows = xin[p]
-        gate_act = jnp.dot(rows, wg[...], preferred_element_type=F32)
-        up_act = jnp.dot(rows, wu[...], preferred_element_type=F32)
+        gate_act = up_act = None
+        for ch in range(2):
+            hc = half[ch]
+            mgot(xin.at[p, rest, hc], 66 + 2 * p + ch)
+            rows = xin[p, :, hc]
+            ga = jnp.dot(rows, wg[hc, :], preferred_element_type=F32)
+            ua = jnp.dot(rows, wu[hc, :], preferred_element_type=F32)
+            gate_act, up_act = (ga, ua) if ch == 0 else (gate_act + ga, up_act + ua)
         hidden = (gate_act / (1.0 + jnp.exp(-gate_act)) * up_act).astype(BF)
 
         for ch in range(2):
@@ -470,7 +495,7 @@
                 pbuf[p, :, cols] = out
                 rbuf[p, 0:16, cols] = out[0:16, :]
 
-            for o in (2, 6, 4, 5, 3, 7, 1):
+            for o in (4, 5, 3, 2, 6, 7, 1):
                 sl = pl.ds(16 * o, 16)
                 mgo(pbuf.at[p, sl, half[ch]], rbuf.at[p, sl, half[ch]], 30 + 2 * p + ch, xdev(me - o), note=False)
 
@@ -516,35 +541,27 @@
         cp.wait()
     for k in (2, 3):
         fin2[g_of[k]] = jnp.zeros((64, 2048), BF)
-    mgot(land.at[1], 9)
-    exchange(0)
-    mgot(land.at[2], 10)
+    exchange(0, 1)
     fwd(2)
-    mgot(land.at[4], 8)
-    exchange(1)
+    exchange(1, 4)
     expert(0)
-    mgot(land.at[3], 11)
     fwd(3)
-    fwd(1)
+    fwd(1, False)
     expert(1)
-    mgot(land.at[6], 13)
-    mgot(land.at[7], 14)
-    exchange(2)
-    merge(0, 0)
-    merge(0, 1)
-    merge(1, 0)
-    merge(1, 1)
-    mgot(land.at[5], 12)
-    exchange(3)
+    exchange(2, 6, 7)
+    for p in (0, 1):
+        merge(p, 0)
+        merge(p, 1)
+    exchange(3, 5)
     expert(2)
+    merge(2, 0)
     expert(3)
-    merge(2, 0)
     merge(2, 1)
     merge(3, 0)
     total(3, 0)
+    total(2, 0)
     merge(3, 1)
     total(3, 1)
-    total(2, 0)
     total(2, 1)
     for ch in range(2):
         hc = half[ch]
@@ -565,8 +582,8 @@
     for d in pending:
         d.wait_send()
     for p in range(4):
-        mrc(xbuf.at[p, rest], xbuf.at[p, rest], 15 + p, partner).wait_send()
         for ch in range(2):
+            mrc(xbuf.at[p, rest, half[ch]], xbuf.at[p, rest, half[ch]], 66 + 2 * p + ch, partner).wait_send()
             mrc(pbuf.at[p, rest, half[ch]], pbuf.at[p, rest, half[ch]], 30 + 2 * p + ch, partner).wait_send()
 
 
@@ -622,7 +639,7 @@
             pltpu.VMEM((2048, 512), BF),
             pltpu.VMEM((2048, 512), BF),
             pltpu.VMEM((512, 2048), BF),
-            dma((84,)), dma((84,)), dma((52,)), dma((52,)), dma((5,)),
+            dma((84,)), dma((84,)), dma((74,)), dma((74,)), dma((5,)),
         ],
         compiler_params=pltpu.CompilerParams(
             collective_id=0, has_side_effects=True, vmem_limit_bytes=62 * 2**20

time: 135 us -> 130 us (0.963)
  Pallas kernels: 131 us -> 127 us
    pallas_call x1, Pallas kernels: 131 us -> 127 us  [layer(): pl.pallas_call(layer_kernel, out_shape=jax.ShapeDtypeStruct((256, 2048),...]
where the time goes in v5:
time: 130 us; the launch traced here: 129 us
  Pallas kernels  127 us (98%)
  local copies, waits for them, and re-layouts  2.3 us (2%)
    pallas_call x1, Pallas kernels, layer(): pl.pallas_call(layer_kernel, out_shape=jax.ShapeDtypeStruct((256, 2048),...  127 us

profile of v5, /device:TPU:2, one launch (start us, length us, event | category | flops | bytes accessed | tf_op | source)
XLA Modules:
  0.0 129.3 jit_solution(3082044842332662451)
XLA Ops:
  0.0 127.0 %layer.1 = bf16[256,2048]{1,0:T(8,128)(2,1)} custom-call(bf16[1024,512]{1,0:T(8,128)(2,1)} %q_ref.1, bf16[1024,128]{1,0:T(8,128)(2,1)} %k_ref.1, bf16[1024,128]{1,0:T(8,128)(2,1)} %v_ref.1, s32[8,1,128]{2,1,0:T(1,128)} %bitcast.5, f32[8]{0:T(128)} %sink_ref.1, f32[1,2048]{1,0:T(1,128)} %bitcast.4, s32[2,256]{1,0:T(2,128)} %bitcast.6, f32[2,256]{1,0:T(2,128)} %bitcast.7, ...), custom_call_target="tpu_custom_call" | custom-call | tf_op jit(solution)/shard_map/layer/pallas_call | solution.py:598
  127.0 2.3 %copy.15 = bf16[256,2048]{1,0:T(8,128)(2,1)} copy(bf16[256,2048]{1,0:T(8,128)(2,1)} %layer.1) | data formatting | bytes 2097152

commit v6 on v5

--- a/solution.py
+++ b/solution.py
@@ -185,10 +185,10 @@
     mine = rows_a(x, c, 0, 32)
     mine_lo, mine_hi = rows_a(x, c, 0, 16), rows_a(x, c, 16, 16)
     mine_b = rows_b(z, c)
+    go(w_own.at[mine_b], wall.at[0, mine_b], 30, tps[1])
+    go(w_own.at[mine_b], wall.at[1, mine_b], 31, tps[3])
     go(w_own.at[mine], wall.at[0, mine], 6, tps[1])
     go(w_own.at[mine], wall.at[1, mine], 7, tps[3])
-    go(w_own.at[mine_b], wall.at[0, mine_b], 30, tps[1])
-    go(w_own.at[mine_b], wall.at[1, mine_b], 31, tps[3])
 
     for o in range(1, 8):
         zz = lax.rem(z + o, 8)
@@ -312,43 +312,43 @@
         go(ref, ref, 15 + 2 * sh, x_prev)
 
     pair_of_blocks(0, att, 0)
+    got(wall.at[0, mine_b], 30)
+    go(wall.at[0, mine_b, left], wall.at[2, mine_b, left], 32, tps[1])
+    got(wall.at[1, mine_b], 31)
+    go(wall.at[1, mine_b, right], wall.at[2, mine_b, right], 33, tps[3])
+    zsend(1, 0)
     got(wall.at[0, mine], 6)
     go(wall.at[0, mine_lo], wall.at[2, mine_lo], 8, tps[1])
     got(wall.at[1, mine], 7)
     go(wall.at[1, mine_hi], wall.at[2, mine_hi], 9, tps[3])
-    got(wall.at[0, mine_b], 30)
-    go(wall.at[0, mine_b, left], wall.at[2, mine_b, left], 32, tps[1])
-    got(wall.at[1, mine_b], 31)
-    go(wall.at[1, mine_b, right], wall.at[2, mine_b, right], 33, tps[3])
     xsend(0)
-    zsend(1, 0)
     pair_of_blocks(1, att, 1)
     send_att(0)
+    got(wall.at[2, mine_b, left], 32)
+    got(wall.at[2, mine_b, right], 33)
+    zsend(1, 1)
+    zgot(1, 0)
+    zsend(2, 0)
     got(wall.at[2, mine_lo], 8)
     got(wall.at[2, mine_hi], 9)
-    got(wall.at[2, mine_b, left], 32)
-    got(wall.at[2, mine_b, right], 33)
     xsend(1)
-    zsend(1, 1)
     for sh in range(2):
         xsib(sh, 0)
         zsib(sh, 0)
-    zgot(1, 0)
-    zsend(2, 0)
     pair_of_blocks(2, att, 2)
     send_att(1)
-    xforward(0)
     zgot(1, 1)
     zsend(2, 1)
     zgot(2, 0)
     zsend(3, 0)
+    xforward(0)
     pair_of_blocks(3, regr, 0)
     send_att(2)
-    xforward(1)
     zgot(2, 1)
     zsend(3, 1)
     zgot(3, 0)
     zsend(4, 0)
+    xforward(1)
     for sh in range(2):
         xsib(sh, 1, 2)
         zsib(sh, -1, 1, -2, 2)

time: 130 us -> 128 us (0.985)
  Pallas kernels: 127 us -> 125 us
    pallas_call x1, Pallas kernels: 127 us -> 125 us  [layer(): pl.pallas_call(layer_kernel, out_shape=jax.ShapeDtypeStruct((256, 2048),...]
where the time goes in v6:
time: 128 us; the launch traced here: 127 us
  Pallas kernels  125 us (98%)
  local copies, waits for them, and re-layouts  2.3 us (2%)
    pallas_call x1, Pallas kernels, layer(): pl.pallas_call(layer_kernel, out_shape=jax.ShapeDtypeStruct((256, 2048),...  125 us

profile of v6, /device:TPU:2, one launch (start us, length us, event | category | flops | bytes accessed | tf_op | source)
XLA Modules:
  0.0 127.2 jit_solution(11889160741830788697)
XLA Ops:
  0.0 124.9 %layer.1 = bf16[256,2048]{1,0:T(8,128)(2,1)} custom-call(bf16[1024,512]{1,0:T(8,128)(2,1)} %q_ref.1, bf16[1024,128]{1,0:T(8,128)(2,1)} %k_ref.1, bf16[1024,128]{1,0:T(8,128)(2,1)} %v_ref.1, s32[8,1,128]{2,1,0:T(1,128)} %bitcast.5, f32[8]{0:T(128)} %sink_ref.1, f32[1,2048]{1,0:T(1,128)} %bitcast.4, s32[2,256]{1,0:T(2,128)} %bitcast.6, f32[2,256]{1,0:T(2,128)} %bitcast.7, ...), custom_call_target="tpu_custom_call" | custom-call | tf_op jit(solution)/shard_map/layer/pallas_call | solution.py:598
  124.9 2.3 %copy.15 = bf16[256,2048]{1,0:T(8,128)(2,1)} copy(bf16[256,2048]{1,0:T(8,128)(2,1)} %layer.1) | data formatting | bytes 2097152
